TPU v7x, 128 devices: a whole 4x4x4 slice. The times are simulated.
128 devices in a mesh: sp: 16 (over z, x), dp: 8 (over y, core).
Axes of the slice: x: 4, y: 4, z: 4, core: 2. Of those that a mesh axis runs over, the one named last changes fastest.
Arguments:
- skip_stream_entering: bfloat16 [8, 2048, 2048], P('dp', 'sp'), may hold values from -6 to 6
- mapped_probe_matrix: bfloat16 [8, 2048, 2048], P('dp', 'sp'), may hold values from -6 to 6
- mapped_lookup_matrix: bfloat16 [8, 2048, 2048], P('dp', 'sp'), may hold values from -6 to 6
- mapped_content_matrix: bfloat16 [8, 2048, 4096], P('dp', 'sp'), may hold values from -6 to 6
- retention_preactivation: bfloat16 [8, 2048, 2048], P('dp', 'sp'), may hold values from -4 to 12
- extra_shrinkage: float32 [8, 16, 2048], P('dp', 'sp'), may hold values from -0.6932 to 0
- attention_group_scale: float32 [4096], replicated, may hold values from 0.1 to 1.9
- final_projection_matrix: bfloat16 [4096, 2048], P(None, 'dp'), may hold values from -0.09375 to 0.09375
- blender_branch_scale: float32 [2048], replicated, may hold values from 0.1 to 1.9
- specialist_prenormal_scale: float32 [2048], replicated, may hold values from 0.1 to 1.9
- specialist_switch_matrix: bfloat16 [128, 2048, 1024], P(('sp', 'dp')), may hold values from -0.125 to 0.125
- specialist_expand_matrix: bfloat16 [128, 2048, 1024], P(('sp', 'dp')), may hold values from -0.125 to 0.125
- specialist_contract_matrix: bfloat16 [128, 1024, 2048], P(('sp', 'dp')), may hold values from -0.1875 to 0.1875
- specialist_branch_scale: float32 [2048], replicated, may hold values from 0.1 to 1.9
- assigned_specialists: int32 [8, 2048, 2], P('dp', 'sp'), may hold values from 0 to 127, all different within a row; in each aligned block of 128 rows (0 to 127, 128 to 255, ..., all dimensions but the last counted through in order) at most 3 rows name the same one
- dispatcher_logits: float32 [8, 2048, 2], P('dp', 'sp'), may hold values from 0.2 to 1
Outputs:
- layer_out: bfloat16 [8, 2048, 2048], P('dp', 'sp')
Inputs may be any that keep to these rules, and one draw needn't show every extreme that they name: `assigned_specialists`: in the rows of one device no expert is named more than 3 times; in every draw some expert reaches 3 on some device.
All inputs are finite; a program needn't handle non-finite values.
Results may differ from a plain program's by a relative error of at most 0.013.
Values may be sent and summed in bfloat16 or wider, within the bound.
A program may use at most 128 MiB of HBM per device.

v0:
```python
import jax
import jax.numpy as jnp
from jax import lax
from jax.sharding import PartitionSpec as P

D = 2048
ATTENTION_GROUPS = 16
KEY_WIDTH = 128
DV = 256
TOP = 2
BLOCK = 64


epsilon = 1e-06
softness_factor = 16.0


def sent_together(arrays, axis, split_dim, concat_dim, along):
    ends, at = ([], 0)
    for a in arrays[:-1]:
        at += a.shape[along]
        ends.append(at)
    both = jnp.concatenate(arrays, axis=along)
    return tuple(
        jnp.split(
            lax.all_to_all(both, axis, split_axis=split_dim, concat_axis=concat_dim, tiled=True),
            ends,
            axis=along,
        )
    )


def split_up(value, dim, size):
    before, after = (value.shape[:dim], value.shape[dim + 1 :])
    return jnp.moveaxis(value.reshape(*before, size, -1, *after), dim, 0)


def in_order(pieces, dim):
    shape = list(pieces.shape[1:])
    shape[dim] *= pieces.shape[0]
    return jnp.moveaxis(pieces, 0, dim).reshape(shape)


def one_exchange(value, axis, axes, splits, concats):
    sizes = [lax.axis_size(a) for a in axes]
    pieces = split_up(value, splits[0], sizes[0])
    pieces = jnp.moveaxis(split_up(pieces, splits[1] + 1, sizes[1]), 0, 1)
    inside = pieces.shape[2:]
    pieces = pieces.reshape(-1, *inside)
    pieces = lax.all_to_all(pieces, axis, split_axis=0, concat_axis=0, tiled=True)
    pieces = in_order(pieces.reshape(*sizes, *inside), concats[0] + 1)
    return in_order(pieces, concats[1])


def rms_scale(values, gain):
    mean_square = jnp.mean(values * values, axis=-1, keepdims=True)
    return values * lax.rsqrt(mean_square + epsilon) * gain


def combine_states(earlier, later):
    return (earlier[0] * later[0], later[0][..., None] * earlier[1] + later[1])


def block_attention(query_f, key_f, value_f, shrink_exponent):
    length_value, head_count, key_dim = query_f.shape
    value_dim = value_f.shape[-1]
    block_count = length_value // BLOCK
    query_blocks = query_f.reshape(block_count, BLOCK, head_count, key_dim)
    key_blocks = key_f.reshape(block_count, BLOCK, head_count, key_dim)
    value_blocks = value_f.reshape(block_count, BLOCK, head_count, value_dim)
    within = jnp.cumsum(shrink_exponent.reshape(block_count, BLOCK, head_count, key_dim), axis=1)
    block_end = within[:, -1]
    lifted = query_blocks * jnp.exp(within)
    lowered = key_blocks * jnp.exp(-within)
    scores = jnp.einsum("nthk,nshk->nhts", lifted, lowered)
    causal = jnp.arange(BLOCK)[:, None] >= jnp.arange(BLOCK)[None, :]
    scores = jnp.where(causal, scores, 0.0)
    inside = jnp.einsum("nhts,nshv->nthv", scores, value_blocks)
    carried_keys = key_blocks * jnp.exp(block_end[:, None] - within)
    updates = jnp.einsum("nshk,nshv->nhkv", carried_keys, value_blocks)
    decays = jnp.exp(block_end)
    total_decay, states = lax.associative_scan(combine_states, (decays, updates), axis=0)
    entering = jnp.concatenate([jnp.zeros_like(states[:1]), states[:-1]], axis=0)
    across = jnp.einsum("nthk,nhkv->nthv", lifted, entering)
    outputs = (inside + across).reshape(length_value, head_count, value_dim)
    offsets = jnp.cumsum(block_end, axis=0) - block_end
    reached = (query_blocks * jnp.exp(within + offsets[:, None])).reshape(
        length_value, head_count, key_dim
    )
    return (outputs, total_decay[-1], states[-1], reached)


def shards(
    skip_stream_entering,
    mapped_probe_matrix,
    mapped_lookup_matrix,
    mapped_content_matrix,
    retention_preactivation,
    extra_shrinkage,
    attention_group_scale,
    final_projection_matrix,
    blender_branch_scale,
    specialist_prenormal_scale,
    specialist_switch_matrix,
    specialist_expand_matrix,
    specialist_contract_matrix,
    specialist_branch_scale,
    assigned_specialists,
    dispatcher_logits,
):
    tok_rows = mapped_probe_matrix.shape[1]
    sp_count = lax.axis_size("sp")
    dp_count = lax.axis_size("dp")
    query_local = mapped_probe_matrix[0].reshape(tok_rows, ATTENTION_GROUPS, KEY_WIDTH)
    key_local = mapped_lookup_matrix[0].reshape(tok_rows, ATTENTION_GROUPS, KEY_WIDTH)
    value_local = mapped_content_matrix[0].reshape(tok_rows, ATTENTION_GROUPS, DV)
    decay_local = retention_preactivation[0].reshape(tok_rows, ATTENTION_GROUPS, KEY_WIDTH)
    arrived = sent_together((query_local, key_local, value_local, decay_local), "sp", 1, 0, 2)
    query_head, key_head, value_head, head_decay = arrived
    own_heads = query_head.shape[1]
    shrink_exponent = jax.nn.log_sigmoid(head_decay.astype(jnp.float32)) / softness_factor
    shrink_exponent = shrink_exponent + jnp.transpose(extra_shrinkage[0])[:, :, None]
    outputs = block_attention(
        query_head.astype(jnp.float32) * KEY_WIDTH ** (-0.5),
        key_head.astype(jnp.float32),
        value_head.astype(jnp.float32),
        shrink_exponent,
    )[0]
    offset = lax.axis_index("sp") * (own_heads * DV)
    gains = lax.dynamic_slice_in_dim(attention_group_scale, offset, own_heads * DV).reshape(
        own_heads, DV
    )
    normed = rms_scale(outputs, gains).astype(jnp.bfloat16)
    attention_group_result = lax.all_to_all(normed, "sp", split_axis=0, concat_axis=1, tiled=True)
    flat_heads = attention_group_result.reshape(tok_rows, ATTENTION_GROUPS * DV)
    projected = jnp.dot(
        flat_heads,
        lax.all_gather(final_projection_matrix, "dp", axis=1, tiled=True),
        preferred_element_type=jnp.float32,
    ).astype(jnp.bfloat16)
    stream = skip_stream_entering[0].astype(jnp.float32)
    residual = (stream + rms_scale(projected.astype(jnp.float32), blender_branch_scale)).astype(
        jnp.bfloat16
    )
    expert_in = rms_scale(residual.astype(jnp.float32), specialist_prenormal_scale).astype(
        jnp.bfloat16
    )
    expert_total = sp_count * dp_count
    capacity = max(2, 5 * tok_rows * TOP // (3 * expert_total))
    chosen = assigned_specialists[0].reshape(-1)
    pair_total = chosen.shape[0]
    onehot = (chosen[:, None] == jnp.arange(expert_total, dtype=jnp.int32)[None, :]).astype(
        jnp.int32
    )
    ranks = jnp.sum((jnp.cumsum(onehot, axis=0) - onehot) * onehot, axis=1)
    slots = chosen * capacity + ranks
    table = jnp.full((expert_total * capacity,), pair_total, jnp.int32)
    table = table.at[slots].set(jnp.arange(pair_total, dtype=jnp.int32))
    padded = jnp.concatenate([expert_in, jnp.zeros((1, D), jnp.bfloat16)], axis=0)
    outgoing = padded[table // TOP].reshape(expert_total, capacity, D)
    grid = outgoing.reshape(sp_count, dp_count, capacity, D)
    arrived_grid = one_exchange(grid, ("sp", "dp"), ("sp", "dp"), (0, 1), (0, 1))
    row_block = arrived_grid.reshape(-1, D)
    gate_part = jnp.dot(row_block, specialist_switch_matrix[0], preferred_element_type=jnp.float32)
    up_part = jnp.dot(row_block, specialist_expand_matrix[0], preferred_element_type=jnp.float32)
    hidden_units = (jax.nn.silu(gate_part) * up_part).astype(jnp.bfloat16)
    result = jnp.dot(
        hidden_units, specialist_contract_matrix[0], preferred_element_type=jnp.float32
    )
    processed = result.astype(jnp.bfloat16).reshape(arrived_grid.shape)
    returned = one_exchange(processed, ("sp", "dp"), ("sp", "dp"), (0, 1), (0, 1))
    flat_back = returned.reshape(expert_total * capacity, D)
    pair_rows = flat_back[slots].reshape(tok_rows, TOP, D)
    weights = dispatcher_logits[0]
    weights = weights / jnp.sum(weights, axis=1, keepdims=True)
    combined = jnp.sum(pair_rows.astype(jnp.float32) * weights[:, :, None], axis=1)
    layer_out = residual.astype(jnp.float32) + rms_scale(combined, specialist_branch_scale)
    return layer_out.astype(jnp.bfloat16)[None]


def solution(mesh):
    return jax.shard_map(
        shards,
        mesh=mesh,
        in_specs=(
            P("dp", "sp", None),
            P("dp", "sp", None),
            P("dp", "sp", None),
            P("dp", "sp", None),
            P("dp", "sp", None),
            P("dp", "sp", None),
            P(),
            P(None, "dp"),
            P(),
            P(),
            P(("sp", "dp"), None, None),
            P(("sp", "dp"), None, None),
            P(("sp", "dp"), None, None),
            P(),
            P("dp", "sp", None),
            P("dp", "sp", None),
        ),
        out_specs=P("dp", "sp", None),
        check_vma=False,
    )
```

profile of v0, /device:TPU:1, one launch (start us, length us, event | category | flops | bytes accessed | tf_op | source)
XLA Modules:
  0.0 298.4 jit_solution(1398296996152553619)
XLA Ops:
  6.5 0.7 all-gather.2.cloned.1.call-update
  7.3 0.5 copy-done.8
  8.4 0.4 copy-done.12
  9.4 0.5 copy-done.14
  10.1 1.7 pad_maximum_fusion
  11.8 8.5 %all-to-all-start = ((bf16[128,16,640]{2,0,1:T(8,128)(2,1)}), bf16[128,16,640]{2,0,1:T(8,128)(2,1)S(1)}, u32[]{:S(2)}, u32[]{:S(2)}) async-start(bf16[128,16,640]{2,0,1:T(8,128)(2,1)} %pad_maximum_fusion), calls=%async_computation | async-start | bytes 5242880 | tf_op jit(solution)/shard_map/all_to_all | solution.py:26
  21.1 0.8 dynamic_slice.3
  21.8 37.6 %all-to-all-done = bf16[128,16,640]{2,0,1:T(8,128)(2,1)S(1)} async-done(((bf16[128,16,640]{2,0,1:T(8,128)(2,1)}), bf16[128,16,640]{2,0,1:T(8,128)(2,1)S(1)}, u32[]{:S(2)}, u32[]{:S(2)}) %all-to-all-start) | async-done | bytes 2621472 | tf_op jit(solution)/shard_map/all_to_all | solution.py:26
  59.5 1.0 split.16
  60.5 1.8 convert_multiply_fusion.2
  62.3 0.6 fusion.40
  63.6 2.5 fusion.35
  66.1 0.8 fusion.36
  67.2 1.6 copy-done
  68.8 0.7 slice.172
  69.7 0.9 copy-done.5
  71.0 0.7 pad_maximum_fusion.4
  71.8 2.5 pad.35
  74.2 0.7 pad_add_fusion
  75.0 2.5 pad.36
  77.5 2.1 add.178
  79.6 4.2 %pad.38 = f32[8,1,128,256]{3,2,0,1:T(8,128)} pad(f32[4,1,128,256]{3,2,0,1:T(8,128)} %add.178, f32[]{:T(128)} %constant.27.clone.1), padding=1_0_1x0_0_0x0_0_0x0_0_0 | pad | bytes 1572868 | tf_op jit(solution)/shard_map/pad | solution.py:82
  83.7 1.4 fusion.52
  85.1 0.9 pad_maximum_fusion.3
  86.0 4.1 %pad.37 = f32[8,1,128,256]{3,2,0,1:T(8,128)} pad(f32[4,1,128,256]{3,2,0,1:T(8,128)} %pad_maximum_fusion.3, f32[]{:T(128)} %constant.27.clone.1), padding=0_1_1x0_0_0x0_0_0x0_0_0 | pad | bytes 1572868 | tf_op jit(solution)/shard_map/pad | solution.py:82
  90.1 2.8 add.180
  93.3 0.6 copy-done.11
  93.8 1.1 pad_maximum_fusion.2
  94.9 4.0 %pad.39 = f32[16,1,128,256]{3,2,0,1:T(8,128)S(1)} pad(f32[8,1,128,256]{3,2,0,1:T(8,128)} %pad_maximum_fusion.2, f32[]{:T(128)} %constant.27.clone.1), padding=0_1_1x0_0_0x0_0_0x0_0_0 | pad | bytes 3145732 | tf_op jit(solution)/shard_map/pad | solution.py:82
  98.9 6.5 %pad.40 = f32[16,1,128,256]{3,2,0,1:T(8,128)} pad(f32[8,1,128,256]{3,2,0,1:T(8,128)} %add.180, f32[]{:T(128)} %constant.27.clone.1), padding=1_0_1x0_0_0x0_0_0x0_0_0 | pad | bytes 3145732 | tf_op jit(solution)/shard_map/pad | solution.py:82
  105.4 3.2 %add.182 = f32[16,1,128,256]{3,2,0,1:T(8,128)} add(f32[16,1,128,256]{3,2,0,1:T(8,128)S(1)} %pad.39, f32[16,1,128,256]{3,2,0,1:T(8,128)} %pad.40) | non-fusion elementwise | flops 524288 | bytes 6291456 | tf_op jit(solution)/shard_map/add | solution.py:82
  108.6 11.4 %pad.86 = f32[32,1,128,256]{3,2,0,1:T(8,128)} pad(f32[16,1,128,256]{3,2,0,1:T(8,128)} %add.182, f32[]{:T(128)} %constant.27.clone.1), padding=1_0_1x0_0_0x0_0_0x0_0_0 | pad | bytes 6291460
  120.0 0.9 slice_bitcast_fusion
  120.9 2.6 fusion.16
  123.7 7.2 %pad.58 = f32[31,1,128,256]{3,2,0,1:T(8,128)} pad(f32[16,1,128,256]{3,2,0,1:T(8,128)S(1)} %pad_maximum_fusion.1, f32[]{:T(128)} %constant.27.clone.1), padding=0_0_1x0_0_0x0_0_0x0_0_0 | pad | bytes 6160388 | tf_op jit(solution)/shard_map/slice | solution.py:83
  130.9 1.9 fusion.22
  132.9 4.1 %slice_add_fusion.5 = bf16[31,1,128,256]{3,2,0,1:T(8,128)(2,1)S(1)} fusion(f32[31,1,128,256]{3,2,0,1:T(8,128)} %pad.58, f32[32,1,128,256]{3,2,0,1:T(8,128)} %pad.86), kind=kLoop, calls=%fused_computation.121 | loop fusion | flops 2031616 | bytes 10158080 | tf_op jit(solution)/shard_map/add | solution.py:82
  136.9 1.9 fusion.15
  138.9 1.9 fusion.14
  140.9 0.5 broadcast.223
  141.4 1.4 reduce.3
  142.8 1.1 reshape.349
  144.0 3.7 %all-to-all-start.1 = ((bf16[16,2,16384]{2,1,0:T(2,128)(2,1)}), bf16[16,2,16384]{2,1,0:T(2,128)(2,1)S(1)}, u32[]{:S(2)}, u32[]{:S(2)}) async-start(bf16[16,2,16384]{2,1,0:T(2,128)(2,1)} %reshape.349), calls=%async_computation.1 | async-start | bytes 2097152 | tf_op jit(solution)/shard_map/all_to_all | solution.py:134
  148.3 1.6 scatter_custom_fusion
  149.9 12.8 %all-to-all-done.1 = bf16[16,2,16384]{2,1,0:T(2,128)(2,1)S(1)} async-done(((bf16[16,2,16384]{2,1,0:T(2,128)(2,1)}), bf16[16,2,16384]{2,1,0:T(2,128)(2,1)S(1)}, u32[]{:S(2)}, u32[]{:S(2)}) %all-to-all-start.1) | async-done | bytes 1048608 | tf_op jit(solution)/shard_map/all_to_all | solution.py:134
  162.7 1.0 reshape.350
  163.9 0.7 copy.91
  164.7 8.3 %multiply_reduce_fusion.2 = (f32[128]{0:T(128)S(1)}, f32[128,2048]{1,0:T(8,128)S(1)}) fusion(bf16[128,4096]{0,1:T(8,128)(2,1)S(1)} %bitcast.154, bf16[4096,2048]{1,0:T(8,128)(2,1)} %all-gather.2.cloned.1.call-done), kind=kOutput, calls=%fused_computation.58 | convolution fusion | flops 2148532224 | bytes 18874880 | tf_op jit(solution)/shard_map/dot_general | solution.py:136
  173.0 0.4 fusion.23
  173.9 3.1 %gather_fusion = bf16[384,2048]{1,0:T(8,128)(2,1)} fusion(bf16[129,2048]{1,0:T(8,128)(2,1)S(1)} %concatenate.27, s32[1024]{0:T(1024)S(1)} %pad_clamp_fusion.1), kind=kCustom, calls=%fused_computation | custom fusion | bytes 3147264 | tf_op jit(solution)/shard_map/gather | solution.py:160
  177.0 4.0 %reshape_transpose_transpose_reshape_reshape_reshape_reshape.3 = bf16[128,1,1,3,2048]{4,3,0,2,1:T(4,128)(2,1)S(1)} reshape(bf16[384,2048]{1,0:T(8,128)(2,1)} %gather_fusion) | data formatting | bytes 3145728 | tf_op jit(solution)/shard_map/reshape;transpose;transpose;reshape;reshape;reshape;reshape | solution.py:49
  181.0 38.3 %all_to_all.43 = bf16[128,1,1,3,2048]{4,3,2,1,0:T(4,128)(2,1)} all-to-all(bf16[128,1,1,3,2048]{4,3,2,1,0:T(4,128)(2,1)S(1)} %bitcast.152), channel_id=1, replica_groups=mesh['sp'=16,'dp'=8] {'sp','dp'}, dimensions={0} | all-to-all | bytes 3145728 | tf_op jit(solution)/shard_map/all_to_all | solution.py:50
  219.3 3.9 %reshape_reshape.6 = bf16[384,2048]{1,0:T(8,128)(2,1)S(1)} reshape(bf16[16,8,1,3,2048]{4,3,1,0,2:T(4,128)(2,1)} %bitcast.153) | data formatting | bytes 3145728 | tf_op jit(solution)/shard_map/reshape;reshape | solution.py:163
  223.2 5.1 %fusion.4 = f32[384,1024]{1,0:T(8,128)} fusion(bf16[384,2048]{1,0:T(8,128)(2,1)S(1)} %reshape_reshape.6, bf16[1,2048,1024]{2,1,0:T(8,128)(2,1)} %param.26), kind=kOutput, calls=%fused_computation.7 | convolution fusion | flops 1610612736 | bytes 7340032 | tf_op jit(solution)/shard_map/dot_general | solution.py:164
  228.3 8.6 %fusion.9 = bf16[384,2048]{1,0:T(8,128)(2,1)} fusion(bf16[1,1024,2048]{2,1,0:T(8,128)(2,1)} %param.28, f32[384,1024]{1,0:T(8,128)} %fusion.4, bf16[384,2048]{1,0:T(8,128)(2,1)S(1)} %reshape_reshape.6, bf16[1,2048,1024]{2,1,0:T(8,128)(2,1)} %param.27), kind=kOutput, calls=%fused_computation.13 | convolution fusion | flops 3224371200 | bytes 13107200 | tf_op jit(solution)/shard_map/dot_general | solution.py:167
  236.9 5.2 %reshape_transpose_transpose_reshape_reshape_reshape.3 = bf16[128,1,1,3,2048]{4,3,0,2,1:T(4,128)(2,1)} reshape(bf16[384,2048]{1,0:T(8,128)(2,1)} %fusion.9) | data formatting | bytes 3145728 | tf_op jit(solution)/shard_map/reshape;transpose;transpose;reshape;reshape;reshape | solution.py:49
  242.1 4.9 %all-to-all-start.3 = ((bf16[128,1,1,3,2048]{4,3,2,1,0:T(4,128)(2,1)}), bf16[128,1,1,3,2048]{4,3,2,1,0:T(4,128)(2,1)S(1)}, u32[]{:S(2)}, u32[]{:S(2)}) async-start(bf16[128,1,1,3,2048]{4,3,2,1,0:T(4,128)(2,1)} %bitcast.151), calls=%async_computation.3 | async-start | bytes 4194304 | tf_op jit(solution)/shard_map/all_to_all | solution.py:50
  247.1 30.1 %all-to-all-done.3 = bf16[128,1,1,3,2048]{4,3,2,1,0:T(4,128)(2,1)S(1)} async-done(((bf16[128,1,1,3,2048]{4,3,2,1,0:T(4,128)(2,1)}), bf16[128,1,1,3,2048]{4,3,2,1,0:T(4,128)(2,1)S(1)}, u32[]{:S(2)}, u32[]{:S(2)}) %all-to-all-start.3) | async-done | bytes 1572896 | tf_op jit(solution)/shard_map/all_to_all | solution.py:50
  277.2 1.3 copy-done.4
  278.5 3.9 %reshape_reshape.7 = bf16[384,2048]{1,0:T(8,128)(2,1)S(1)} reshape(bf16[16,8,1,3,2048]{4,3,1,0,2:T(4,128)(2,1)} %bitcast.150) | data formatting | bytes 3145728 | tf_op jit(solution)/shard_map/reshape;reshape | solution.py:172
  282.5 2.3 gather_fusion.1
  284.8 2.4 reshape.321
  287.2 3.2 %multiply_reduce_fusion = f32[128,2048]{1,0:T(8,128)S(1)} fusion(f32[128,2,2048]{2,1,0:T(2,128)S(1)} %reshape.321, f32[128,2]{1,0:T(8,128)S(1)} %copy.99), kind=kLoop, calls=%fused_computation.23 | loop fusion | flops 786432 | bytes 3146752 | tf_op jit(solution)/shard_map/reduce_sum | solution.py:176
  290.5 1.0 fusion.49
  (113 shorter events, 5.9 us)
Async XLA Ops:
  6.5 1.2 copy-start.8
  6.5 158.1 %all-gather.2.cloned.1.call-start = ((), (), s32[]{:S(2)}) async-start(), calls=%async_computation.4 | async-start | bytes 18874368 | tf_op jit(solution)/shard_map/all_gather | solution.py:138
  7.8 1.0 copy-start.12
  8.0 1.1 copy-start.13
  8.8 1.1 copy-start.14
  11.8 8.6 %copy-start.21 = (s32[1,128,2]{1,2,0:T(2,128)S(1)}, s32[1,128,2]{1,2,0:T(2,128)}, u32[]{:S(2)}) copy-start(s32[1,128,2]{1,2,0:T(2,128)} %param.30) | copy-start | bytes 3076
  11.8 47.6 %all-to-all-start = ((bf16[128,16,640]{2,0,1:T(8,128)(2,1)}), bf16[128,16,640]{2,0,1:T(8,128)(2,1)S(1)}, u32[]{:S(2)}, u32[]{:S(2)}) async-start(bf16[128,16,640]{2,0,1:T(8,128)(2,1)} %pad_maximum_fusion), calls=%async_computation | async-start | bytes 5242880 | tf_op jit(solution)/shard_map/all_to_all | solution.py:26
  20.4 40.2 %copy-start.16 = (f32[1,1,2048]{2,1,0:T(1,128)S(1)}, f32[1,1,2048]{2,1,0:T(1,128)}, u32[]{:S(2)}) copy-start(f32[1,1,2048]{2,1,0:T(1,128)} %param.21) | copy-start | bytes 24580
  21.0 38.5 %copy-start.9 = (s32[128,2,128]{0,1,2:T(2,128)}, s32[128,2,128]{0,1,2:T(2,128)S(1)}, u32[]{:S(2)}) copy-start(s32[128,2,128]{0,1,2:T(2,128)S(1)} %fusion.53) | copy-start | bytes 393220
  21.0 41.3 %copy-start.20 = (s32[128,3]{0,1:T(4,128)}, s32[128,3]{0,1:T(4,128)S(1)}, u32[]{:S(2)}) copy-start(s32[128,3]{0,1:T(4,128)S(1)} %reduce-window.9) | copy-start | bytes 4612
  62.3 1.2 copy-start.7
  63.5 2.5 copy-start.1
  66.8 1.9 copy-start
  69.6 1.0 copy-start.5
  77.5 7.7 %slice-start = ((f32[8,1,128,256]{3,2,0,1:T(8,128)}), f32[1,1,128,256]{3,2,0,1:T(8,128)S(1)}, s32[]{:S(2)}) async-start(f32[8,1,128,256]{3,2,0,1:T(8,128)} %copy-done.5), calls=%async_computation.5 | async-start | bytes 262144 | tf_op jit(solution)/shard_map/slice | solution.py:82
  90.1 2.8 copy-start.2
  90.1 2.8 copy-start.3
  92.9 0.9 copy-start.11
  132.9 4.1 %copy-start.6 = (bf16[32,64,128]{2,0,1:T(8,128)(2,1)S(1)}, bf16[32,64,128]{2,0,1:T(8,128)(2,1)}, u32[]{:S(2)}) copy-start(bf16[32,64,128]{2,0,1:T(8,128)(2,1)} %get-tuple-element.13) | copy-start | bytes 1572868
  142.8 4.8 %slice-start.1 = ((s32[128,3]{0,1:T(4,128)}), s32[128,2]{0,1:T(2,128)S(1)}, s32[]{:S(2)}) async-start(s32[128,3]{0,1:T(4,128)} %copy-done.20), calls=%async_computation.6 | async-start | bytes 2048 | tf_op jit(solution)/shard_map/slice.1
  142.8 4.8 %copy-start.10 = (s32[128,2,128]{0,1,2:T(2,128)S(1)}, s32[128,2,128]{0,1,2:T(2,128)}, u32[]{:S(2)}) copy-start(s32[128,2,128]{0,1,2:T(2,128)} %copy-done.9) | copy-start | bytes 393220
  144.0 18.7 %all-to-all-start.1 = ((bf16[16,2,16384]{2,1,0:T(2,128)(2,1)}), bf16[16,2,16384]{2,1,0:T(2,128)(2,1)S(1)}, u32[]{:S(2)}, u32[]{:S(2)}) async-start(bf16[16,2,16384]{2,1,0:T(2,128)(2,1)} %reshape.349), calls=%async_computation.1 | async-start | bytes 2097152 | tf_op jit(solution)/shard_map/all_to_all | solution.py:134
  164.6 8.3 %copy-start.15 = (bf16[1,128,2048]{2,1,0:T(8,128)(2,1)S(1)}, bf16[1,128,2048]{2,1,0:T(8,128)(2,1)}, u32[]{:S(2)}) copy-start(bf16[1,128,2048]{2,1,0:T(8,128)(2,1)} %param.16) | copy-start | bytes 1572868
  164.7 8.3 %copy-start.17 = (f32[2048]{0:T(1024)S(1)}, f32[2048]{0:T(1024)}, u32[]{:S(2)}) copy-start(f32[2048]{0:T(1024)} %param.24) | copy-start | bytes 24580
  172.9 0.7 copy-start.18
  242.1 4.9 %copy-start.22 = (f32[1,128,2]{1,2,0:T(2,128)S(1)}, f32[1,128,2]{1,2,0:T(2,128)}, u32[]{:S(2)}) copy-start(f32[1,128,2]{1,2,0:T(2,128)} %param.31) | copy-start | bytes 3076
  242.1 35.1 %all-to-all-start.3 = ((bf16[128,1,1,3,2048]{4,3,2,1,0:T(4,128)(2,1)}), bf16[128,1,1,3,2048]{4,3,2,1,0:T(4,128)(2,1)S(1)}, u32[]{:S(2)}, u32[]{:S(2)}) async-start(bf16[128,1,1,3,2048]{4,3,2,1,0:T(4,128)(2,1)} %bitcast.151), calls=%async_computation.3 | async-start | bytes 4194304 | tf_op jit(solution)/shard_map/all_to_all | solution.py:50
  277.2 1.3 copy-start.4
  287.2 3.3 %copy-start.19 = (f32[2048]{0:T(1024)S(1)}, f32[2048]{0:T(1024)}, u32[]{:S(2)}) copy-start(f32[2048]{0:T(1024)} %param.29) | copy-start | bytes 24580
Sparse Core Ops, SparseCore 0:
  9.0 93.3 all-gather.1
where the time goes:
time: 300 us; the launch traced here: 298 us
  local copies, waits for them, and re-layouts  84.8 us (28%)
  waiting for transfers between devices  81.2 us (27%)
  blocking collectives  38.3 us (13%)
  other arithmetic  36.5 us (12%)
  matrix products  26.5 us (9%)
  starting transfers between devices  17.1 us (6%)
  between operations  14.1 us (5%)
    all_to_all x1, blocking collectives, one_exchange(): lax.all_to_all(pieces, axis, split_axis=0, concat_axis=0, tiled=True)  38.3 us
    all_to_all x1, waiting for transfers between devices, sent_together(): lax.all_to_all(both, axis, split_axis=split_dim, concat_axis=concat_dim,...  37.6 us
    all_to_all x1, waiting for transfers between devices, one_exchange(): lax.all_to_all(pieces, axis, split_axis=0, concat_axis=0, tiled=True)  30.1 us
    pad x6, local copies, waits for them, and re-layouts, block_attention(): lax.associative_scan(combine_states, (decays, updates), axis=0)  23.8 us
    unnamed x56, local copies, waits for them, and re-layouts  20.9 us
    add x5, other arithmetic, block_attention(): lax.associative_scan(combine_states, (decays, updates), axis=0)  12.9 us
    all_to_all x1, waiting for transfers between devices, shards(): lax.all_to_all(normed, 'sp', split_axis=0, concat_axis=1, tiled=True)  12.8 us
    another operation x2, local copies, waits for them, and re-layouts, one_exchange(): pieces = pieces.reshape(-1, *inside)  9.16 us
  transfers between devices with their start and end apart: 4, of which 3 were waited for; matrix products, arithmetic and copies ran while one was open for 30% of the time, Pallas kernels for 0%

commit v1 on v0

v1 whole, which is shorter than its diff:
```python
import functools
import jax
import jax.numpy as jnp
from jax import lax
from jax.experimental import pallas as pl
from jax.experimental.pallas import tpu as pltpu
from jax.sharding import PartitionSpec as P

MESH = pl.DeviceIdType.MESH
D = 2048
HEADS = 16
KW = 128
DV = 256
FF = 1024
TOK = 128
CAP = 3
EXPERTS = 128
PIECE = 512
HALF = 64
GROUPS = 2
PER = EXPERTS // GROUPS

epsilon = 1e-06
f32 = jnp.float32
bf16 = jnp.bfloat16


def dot_t(a, b, ca, cb):
    return lax.dot_general(a, b, (((ca,), (cb,)), ((), ())), preferred_element_type=f32)


def mixer_kernel(
    q_h, k_h, g_h, v_h, skip_h, spk, w_h, gs, bg, pg,
    res_out, x3_out,
    qv, kv, gv, vv, skipv, spk_in, wall,
    lf, lw, ca, lt, intra, us, ur, dsend, drecv, ss, sr, tall, pj, po, xf,
    lsem, spk_s, spk_r, w_s, w_r, u_s, u_r, d_s, d_r, s_s, s_r, t_s, t_r, p_s, p_r,
):
    sp = lax.axis_index("sp")
    dp = lax.axis_index("dp")
    z, x = sp // 4, sp % 4
    y, c = dp // 2, dp % 2
    partner = (sp, y * 2 + (1 - c))

    def remote(src, dst, s, r, dev):
        return pltpu.make_async_remote_copy(
            src_ref=src, dst_ref=dst, send_sem=s, recv_sem=r, device_id=dev, device_id_type=MESH
        )

    loads = [
        pltpu.make_async_copy(g_h, gv, lsem.at[0]),
        pltpu.make_async_copy(k_h, kv, lsem.at[1]),
        pltpu.make_async_copy(v_h, vv, lsem.at[2]),
        pltpu.make_async_copy(q_h, qv, lsem.at[3]),
        pltpu.make_async_copy(skip_h, skipv, lsem.at[4]),
        pltpu.make_async_copy(w_h, wall.at[0], lsem.at[5]),
    ]
    for one in loads:
        one.start()

    pltpu.make_async_copy(
        spk.at[:, pl.ds(pl.multiple_of(sp * TOK, TOK), TOK)], spk_in.at[sp], spk_r
    ).start()

    @pl.loop(1, HEADS)
    def _(i):
        to = (sp + i) % HEADS
        remote(
            spk.at[:, pl.ds(pl.multiple_of(to * TOK, TOK), TOK)], spk_in.at[sp], spk_s, spk_r, (to, dp)
        ).start()

    base = ((x + z) % 2) * 4
    obase = 4 - base
    up = (sp, ((y + 1) % 4) * 2 + c)
    down = (sp, ((y + 3) % 4) * 2 + c)
    around = [
        (z * 4 + (x + 1) % 4, dp),
        (z * 4 + (x + 3) % 4, dp),
        (((z + 1) % 4) * 4 + x, dp),
        (((z + 3) % 4) * 4 + x, dp),
    ]

    def rows(piece):
        return pl.ds(pl.multiple_of(piece * PIECE, PIECE), PIECE)

    for i in range(4):
        a, b = base + i, base + (i + 2) % 4
        remote(w_h.at[rows(a)], wall.at[1, rows(a)], w_s, w_r.at[0, a], up).start()
        remote(w_h.at[rows(b)], wall.at[3, rows(b)], w_s, w_r.at[2, b], down).start()

    def w_wait(slot, piece):
        there = wall.at[slot, rows(piece)]
        remote(there, there, w_s, w_r.at[slot - 1, piece], partner).wait_recv()

    def w_pass(slot, i):
        piece = base + i
        w_wait(slot, piece)
        there = wall.at[slot, rows(piece)]
        if slot == 1 and i < 2:
            remote(there, wall.at[2, rows(piece)], w_s, w_r.at[1, piece], up).start()
        if slot == 3 and i >= 2:
            remote(there, wall.at[2, rows(piece)], w_s, w_r.at[1, piece], down).start()
        remote(there, there, w_s, w_r.at[slot - 1, piece], around[i]).start()

    row = lax.broadcasted_iota(jnp.int32, (TOK, TOK), 0)
    col = lax.broadcasted_iota(jnp.int32, (TOK, TOK), 1)
    same = (row >= col) & ((row >= HALF) == (col >= HALF))
    cross = (row >= HALF) & (col < HALF)
    first = row < HALF
    tri = jnp.where(same, 1.0, 0.0).astype(bf16)

    for one in loads[:4]:
        one.wait()
    remote(spk_in.at[pl.ds(0, HEADS)], spk_in.at[pl.ds(0, HEADS)], spk_s, spk_r, partner).wait_recv()

    def u_send(h, part):
        rows_u = pl.ds(part * TOK, TOK)
        remote(us.at[h, rows_u], ur.at[sp, rows_u], u_s, u_r.at[part, sp], (h, dp)).start()

    @pl.loop(0, HEADS)
    def _(i):
        h = (sp + 1 + i) % HEADS
        lanes = pl.ds(pl.multiple_of(h * KW, KW), KW)
        g = gv[:, lanes].astype(f32)
        ld = (jnp.minimum(g, 0.0) - jnp.log1p(jnp.exp(-jnp.abs(g)))) * (1.0 / 16.0)
        ld = ld + jnp.broadcast_to(spk_in[h], (TOK, TOK)).T
        hi = ld.astype(bf16)
        rest = ld - hi.astype(f32)
        mid = rest.astype(bf16)
        low = (rest - mid.astype(f32)).astype(bf16)
        b = dot_t(tri, hi, 1, 0) + dot_t(tri, mid, 1, 0) + dot_t(tri, low, 1, 0)
        e1, e2 = b[HALF - 1 : HALF, :], b[TOK - 1 : TOK, :]
        kf = kv[:, lanes].astype(f32)
        qf = qv[:, lanes].astype(f32) * KW ** (-0.5)
        lifted = qf * jnp.exp(b)
        carried = kf * jnp.exp(jnp.where(first, e1, e2) - b)
        ku = carried * jnp.where(first, jnp.exp(e2), 1.0)
        vh = vv[:, pl.ds(pl.multiple_of(h * DV, DV), DV)]
        us[h] = dot_t(vh, ku.astype(bf16), 0, 0).astype(bf16)
        dsend[h] = jnp.exp(e1 + e2)
        lf[h] = lifted.astype(bf16)
        lw[h] = (kf * jnp.exp(-b)).astype(bf16)
        ca[h] = carried.astype(bf16)
        lt[h] = (lifted * jnp.where(first, 1.0, jnp.exp(e1))).astype(bf16)

        @pl.when(i > 0)
        def _():
            u_send((sp + i) % HEADS, 0)

    for part in range(2):
        rows_u = pl.ds(part * TOK, TOK)
        pltpu.make_async_copy(us.at[sp, rows_u], ur.at[sp, rows_u], u_r.at[part, sp]).start()
    pltpu.make_async_copy(dsend.at[sp], drecv.at[sp], d_r).start()

    @pl.loop(1, HEADS)
    def _(i):
        h = (sp + i) % HEADS
        remote(dsend.at[h], drecv.at[sp], d_s, d_r, (h, dp)).start()

    @pl.loop(1, HEADS)
    def _(i):
        u_send((sp + i) % HEADS, 1)

    w_pass(1, 0)
    w_pass(3, 2)

    @pl.loop(0, HEADS)
    def _(h):
        vh = vv[:, pl.ds(pl.multiple_of(h * DV, DV), DV)]
        near = dot_t(lf[h], lw[h], 1, 1)
        far = dot_t(lf[h], ca[h], 1, 1)
        scores = jnp.where(same, near, jnp.where(cross, far, 0.0))
        intra[h] = dot_t(scores.astype(bf16), vh, 1, 0)

    remote(drecv.at[pl.ds(0, HEADS)], drecv.at[pl.ds(0, HEADS)], d_s, d_r, partner).wait_recv()

    for part in range(2):
        rows_u = pl.ds(part * TOK, TOK)

        def step(src, state, rows_u=rows_u, part=part):
            ss[src, rows_u] = state.astype(bf16)

            @pl.when(src != sp)
            def _():
                remote(ss.at[src, rows_u], sr.at[sp, rows_u], s_s, s_r.at[part, sp], (src, dp)).start()

            @pl.when(src == sp)
            def _():
                pltpu.make_async_copy(ss.at[sp, rows_u], sr.at[sp, rows_u], s_r.at[part, sp]).start()

            there = ur.at[src, rows_u]
            remote(there, there, u_s, u_r.at[part, src], partner).wait_recv()
            return state * drecv[src] + ur[src, rows_u].astype(f32)

        lax.fori_loop(0, HEADS, step, jnp.zeros((TOK, KW), f32))
        w_pass(1, part + 1)
        w_pass(3, (part + 3) % 4)

    @pl.loop(0, HEADS)
    def _(i):
        h = (sp + i) % HEADS
        for part in range(2):
            there = sr.at[h, pl.ds(part * TOK, TOK)]
            remote(there, there, s_s, s_r.at[part, h], partner).wait_recv()
        o = intra[h] + dot_t(lt[h], sr[h], 1, 1)
        ms = jnp.mean(o * o, axis=-1, keepdims=True)
        lanes = pl.ds(pl.multiple_of(h * DV, DV), DV)
        tall[pl.ds(0, TOK), lanes] = (o * lax.rsqrt(ms + epsilon) * gs[:, lanes]).astype(bf16)

        @pl.when(i > 0)
        def _():
            prev = pl.ds(pl.multiple_of(((sp + i - 1) % HEADS) * DV, DV), DV)
            remote(tall.at[pl.ds(0, TOK), prev], tall.at[pl.ds(TOK, TOK), prev], t_s, t_r, partner).start()

    last = pl.ds(pl.multiple_of(((sp + HEADS - 1) % HEADS) * DV, DV), DV)
    w_pass(1, 3)
    w_pass(3, 1)
    remote(tall.at[pl.ds(0, TOK), last], tall.at[pl.ds(TOK, TOK), last], t_s, t_r, partner).start()
    loads[4].wait()
    loads[5].wait()
    remote(tall.at[pl.ds(0, TOK)], tall.at[pl.ds(TOK, TOK)], t_s, t_r, partner).wait_recv()

    def project(slot):
        acc = jnp.dot(tall[...], wall[slot], preferred_element_type=f32).astype(bf16)
        shard = ((y + 4 - slot) % 4) * 2 + c
        po[slot] = acc[TOK:]
        pj[shard] = acc[:TOK]
        remote(po.at[slot], pj.at[shard], p_s, p_r, partner).start()

    project(0)
    w_pass(2, 0)
    w_pass(2, 2)
    for i in range(4):
        w_wait(1, obase + i)
    project(1)
    w_pass(2, 1)
    w_pass(2, 3)
    for i in range(4):
        w_wait(3, obase + i)
    project(3)
    for i in range(4):
        w_wait(2, obase + i)
    project(2)
    remote(po.at[pl.ds(0, 4)], pj.at[pl.ds(0, 4)], p_s, p_r, partner).wait_recv()

    total = jnp.zeros((TOK, 1), f32)
    for n in range(8):
        p = pj[n].astype(f32)
        total = total + jnp.sum(p * p, axis=-1, keepdims=True)
    r1 = lax.rsqrt(total * (1.0 / D) + epsilon)
    total = jnp.zeros((TOK, 1), f32)
    for n in range(8):
        lanes = pl.ds(n * 256, 256)
        res = (skipv[:, lanes].astype(f32) + pj[n].astype(f32) * r1 * bg[:, lanes]).astype(bf16)
        res_out[:, lanes] = res
        rf = res.astype(f32)
        total = total + jnp.sum(rf * rf, axis=-1, keepdims=True)
    r2 = lax.rsqrt(total * (1.0 / D) + epsilon)
    for j in range(16):
        lanes = pl.ds(j * 128, 128)
        xf[pl.ds(j, TOK, stride=16), :] = res_out[:, lanes].astype(f32) * r2 * pg[:, lanes]

    @pl.loop(0, 8)
    def _(i):
        at = pl.ds(pl.multiple_of(i * 256, 256), 256)
        x3_out[at, :] = xf[at, :].astype(bf16)

    fifteen = pl.ds(0, HEADS - 1)
    remote(spk_in.at[fifteen], spk_in.at[fifteen], spk_s, spk_r, partner).wait_send()
    remote(drecv.at[fifteen], drecv.at[fifteen], d_s, d_r, partner).wait_send()
    remote(us.at[fifteen], ur.at[fifteen], u_s, u_r.at[0, 0], partner).wait_send()
    remote(ss.at[fifteen], sr.at[fifteen], s_s, s_r.at[0, 0], partner).wait_send()
    remote(tall.at[pl.ds(0, TOK)], tall.at[pl.ds(TOK, TOK)], t_s, t_r, partner).wait_send()
    remote(po.at[pl.ds(0, 4)], pj.at[pl.ds(0, 4)], p_s, p_r, partner).wait_send()
    remote(wall.at[pl.ds(0, 3)], wall.at[pl.ds(0, 3)], w_s, w_r.at[0, 0], partner).wait_send()


def mixer(q, k, g, v, skip, spk, w, gs, bg, pg):
    hbm = pl.BlockSpec(memory_space=pl.ANY)
    vmem = pl.BlockSpec(memory_space=pltpu.VMEM)
    dma = pltpu.SemaphoreType.DMA
    return pl.pallas_call(
        mixer_kernel,
        out_shape=(
            jax.ShapeDtypeStruct((TOK, D), bf16),
            jax.ShapeDtypeStruct((TOK * 16, 128), bf16),
        ),
        in_specs=[hbm] * 5 + [vmem, hbm, vmem, vmem, vmem],
        out_specs=(vmem, vmem),
        scratch_shapes=[
            pltpu.VMEM((TOK, D), bf16),
            pltpu.VMEM((TOK, D), bf16),
            pltpu.VMEM((TOK, D), bf16),
            pltpu.VMEM((TOK, HEADS * DV), bf16),
            pltpu.VMEM((TOK, D), bf16),
            pltpu.VMEM((HEADS, 1, TOK), f32),
            pltpu.VMEM((4, HEADS * DV, 256), bf16),
            pltpu.VMEM((HEADS, TOK, KW), bf16),
            pltpu.VMEM((HEADS, TOK, KW), bf16),
            pltpu.VMEM((HEADS, TOK, KW), bf16),
            pltpu.VMEM((HEADS, TOK, KW), bf16),
            pltpu.VMEM((HEADS, TOK, DV), f32),
            pltpu.VMEM((HEADS, DV, KW), bf16),
            pltpu.VMEM((HEADS, DV, KW), bf16),
            pltpu.VMEM((HEADS, 1, KW), f32),
            pltpu.VMEM((HEADS, 1, KW), f32),
            pltpu.VMEM((HEADS, DV, KW), bf16),
            pltpu.VMEM((HEADS, DV, KW), bf16),
            pltpu.VMEM((2 * TOK, HEADS * DV), bf16),
            pltpu.VMEM((8, TOK, 256), bf16),
            pltpu.VMEM((4, TOK, 256), bf16),
            pltpu.VMEM((TOK * 16, 128), f32),
            dma((6,)),
            dma, dma,
            dma, dma((3, 8)),
            dma, dma((2, HEADS)),
            dma, dma,
            dma, dma((2, HEADS)),
            dma, dma,
            dma, dma,
        ],
        compiler_params=pltpu.CompilerParams(has_side_effects=True, vmem_limit_bytes=56 * 2**20),
        name="mixer",
    )(q, k, g, v, skip, spk, w, gs, bg, pg)


def expert_kernel(
    tab, slots, wts, x3, res, gain, wg_h, wu_h, wd_h,
    out,
    xs, xr, ys, yr, rf, xm, hs, wg, wu, wd,
    wsem, x_s, x_r, y_s, y_r,
):
    sp = lax.axis_index("sp")
    dp = lax.axis_index("dp")
    z, x = sp // 4, sp % 4
    y, c = dp // 2, dp % 2

    def remote(src, dst, s, r, dev):
        return pltpu.make_async_remote_copy(
            src_ref=src, dst_ref=dst, send_sem=s, recv_sem=r, device_id=dev, device_id_type=MESH
        )

    def device(o, sign):
        oc, oz, ox, oy = o // 64, (o // 16) % 4, (o // 4) % 4, o % 4
        if sign < 0:
            oz, ox, oy = 4 - oz, 4 - ox, 4 - oy
        return (((z + oz) % 4) * 4 + (x + ox) % 4, ((y + oy) % 4) * 2 + (c + oc) % 2)

    partner = device(64, 1)
    loads = [
        pltpu.make_async_copy(wg_h, wg, wsem.at[0]),
        pltpu.make_async_copy(wu_h, wu, wsem.at[1]),
        pltpu.make_async_copy(wd_h, wd, wsem.at[2]),
    ]
    for one in loads:
        one.start()

    def pack(grp):
        @pl.loop(0, PER)
        def _(i):
            o = grp * PER + i
            for k in range(CAP):
                xs[o * CAP + k] = x3[tab[o * CAP + k]]

    def send(grp, src, dst, s, r, sign):
        if grp == 0:
            pltpu.make_async_copy(src.at[pl.ds(0, CAP)], dst.at[pl.ds(0, CAP)], r.at[0]).start()

        @pl.loop(1 if grp == 0 else 0, PER)
        def _(i):
            o = grp * PER + i
            at = pl.ds(o * CAP, CAP)
            remote(src.at[at], dst.at[at], s, r.at[grp], device(o, sign)).start()

    pack(0)
    send(0, xs, xr, x_s, x_r, 1)
    for grp in range(1, GROUPS):
        pack(grp)
        send(grp, xs, xr, x_s, x_r, 1)

    R = PER * CAP
    for grp in range(GROUPS):
        at = pl.ds(grp * R, R)
        remote(xr.at[at], xr.at[at], x_s, x_r.at[grp], partner).wait_recv()

        @pl.loop(0, R // 12)
        def _(i):
            rf[pl.ds(pl.multiple_of(i * 192, 192), 192), :] = (
                xr[pl.ds(grp * R + i * 12, 12)].astype(f32).reshape(192, 128)
            )

        for j in range(16):
            xm[:, pl.ds(j * 128, 128)] = rf[pl.ds(j, R, stride=16), :].astype(bf16)
        if grp == 0:
            loads[0].wait()
            loads[1].wait()

        @pl.loop(0, FF // 256)
        def _(n):
            lanes = pl.ds(pl.multiple_of(n * 256, 256), 256)
            a = jnp.dot(xm[...], wg[:, lanes], preferred_element_type=f32)
            b = jnp.dot(xm[...], wu[:, lanes], preferred_element_type=f32)
            hs[:, lanes] = (a * (1.0 / (1.0 + jnp.exp(-a))) * b).astype(bf16)

        if grp == 0:
            loads[2].wait()

        @pl.loop(0, D // 256)
        def _(n):
            lanes = pl.ds(pl.multiple_of(n * 256, 256), 256)
            a = jnp.dot(hs[...], wd[:, lanes], preferred_element_type=f32)
            rf[pl.ds(2 * n, R, stride=16), :] = a[:, :128]
            rf[pl.ds(2 * n + 1, R, stride=16), :] = a[:, 128:]

        @pl.loop(0, R // 12)
        def _(i):
            ys[pl.ds(grp * R + i * 12, 12)] = (
                rf[pl.ds(pl.multiple_of(i * 192, 192), 192), :].reshape(12, 16, 128).astype(bf16)
            )

        send(grp, ys, yr, y_s, y_r, -1)

    for grp in range(GROUPS):
        at = pl.ds(grp * R, R)
        remote(yr.at[at], yr.at[at], y_s, y_r.at[grp], partner).wait_recv()

    @pl.loop(0, TOK // 4)
    def _(i):
        for k in range(4):
            t = i * 4 + k
            one = yr[slots[2 * t]].astype(f32) * wts[2 * t]
            two = yr[slots[2 * t + 1]].astype(f32) * wts[2 * t + 1]
            rf[pl.ds(pl.multiple_of(t * 16, 16), 16), :] = one + two

    total = jnp.zeros((TOK, 1), f32)
    for j in range(16):
        p = rf[pl.ds(j, TOK, stride=16), :]
        total = total + jnp.sum(p * p, axis=-1, keepdims=True)
    r1 = lax.rsqrt(total * (1.0 / D) + epsilon)
    for j in range(16):
        lanes = pl.ds(j * 128, 128)
        p = rf[pl.ds(j, TOK, stride=16), :]
        out[:, lanes] = (res[:, lanes].astype(f32) + p * r1 * gain[:, lanes]).astype(bf16)

    most = pl.ds(0, (EXPERTS - 1) * CAP)
    remote(xs.at[most], xr.at[most], x_s, x_r.at[0], partner).wait_send()
    remote(ys.at[most], yr.at[most], y_s, y_r.at[0], partner).wait_send()


def experts(tab, slots, wts, x3, res, gain, wg, wu, wd):
    hbm = pl.BlockSpec(memory_space=pl.ANY)
    vmem = pl.BlockSpec(memory_space=pltpu.VMEM)
    smem = pl.BlockSpec(memory_space=pltpu.SMEM)
    dma = pltpu.SemaphoreType.DMA
    R = PER * CAP
    return pl.pallas_call(
        expert_kernel,
        out_shape=jax.ShapeDtypeStruct((TOK, D), bf16),
        in_specs=[smem] * 3 + [vmem] * 3 + [hbm] * 3,
        out_specs=vmem,
        scratch_shapes=[
            pltpu.VMEM((EXPERTS * CAP, 16, 128), bf16),
            pltpu.VMEM((EXPERTS * CAP, 16, 128), bf16),
            pltpu.VMEM((EXPERTS * CAP, 16, 128), bf16),
            pltpu.VMEM((EXPERTS * CAP, 16, 128), bf16),
            pltpu.VMEM((R * 16, 128), f32),
            pltpu.VMEM((R, D), bf16),
            pltpu.VMEM((R, FF), bf16),
            pltpu.VMEM((D, FF), bf16),
            pltpu.VMEM((D, FF), bf16),
            pltpu.VMEM((FF, D), bf16),
            dma((3,)),
            dma, dma((GROUPS,)),
            dma, dma((GROUPS,)),
        ],
        compiler_params=pltpu.CompilerParams(has_side_effects=True, vmem_limit_bytes=56 * 2**20),
        name="experts",
    )(tab, slots, wts, x3, res, gain, wg, wu, wd)


def routing(chosen, logits):
    sp = lax.axis_index("sp")
    dp = lax.axis_index("dp")
    z, x, y, c = sp // 4, sp % 4, dp // 2, dp % 2
    esp, edp = chosen // 8, chosen % 8
    o = (
        ((edp % 2 - c + 2) % 2) * 64
        + ((esp // 4 - z + 4) % 4) * 16
        + ((esp % 4 - x + 4) % 4) * 4
        + (edp // 2 - y + 4) % 4
    )
    lane = jnp.arange(EXPERTS, dtype=jnp.int32)
    pick = (o[:, :, None] == lane[None, None, :]).astype(f32)
    named = pick[:, 0] + pick[:, 1]
    time = jnp.arange(TOK, dtype=jnp.int32)
    before = (time[:, None] > time[None, :]).astype(bf16)
    rank = jnp.dot(before, named.astype(bf16), preferred_element_type=f32)
    place = lane.astype(f32)[None, :] * CAP + rank
    slots = jnp.sum(pick * place[:, None, :], axis=-1).astype(jnp.int32).reshape(-1)
    filled = named[:, :, None] * (rank[:, :, None] == jnp.arange(CAP, dtype=f32)[None, None, :])
    tab = jnp.sum(filled * time.astype(f32)[:, None, None], axis=0).astype(jnp.int32).reshape(-1)
    wts = logits / jnp.sum(logits, axis=1, keepdims=True)
    return tab, slots, wts.reshape(-1)


def shards(
    skip_stream_entering,
    mapped_probe_matrix,
    mapped_lookup_matrix,
    mapped_content_matrix,
    retention_preactivation,
    extra_shrinkage,
    attention_group_scale,
    final_projection_matrix,
    blender_branch_scale,
    specialist_prenormal_scale,
    specialist_switch_matrix,
    specialist_expand_matrix,
    specialist_contract_matrix,
    specialist_branch_scale,
    assigned_specialists,
    dispatcher_logits,
):
    tab, slots, wts = routing(assigned_specialists[0], dispatcher_logits[0])
    res, x3 = mixer(
        mapped_probe_matrix[0],
        mapped_lookup_matrix[0],
        retention_preactivation[0],
        mapped_content_matrix[0],
        skip_stream_entering[0],
        extra_shrinkage[0],
        final_projection_matrix,
        attention_group_scale.reshape(1, -1),
        blender_branch_scale.reshape(1, -1),
        specialist_prenormal_scale.reshape(1, -1),
    )
    out = experts(
        tab,
        slots,
        wts,
        x3.reshape(TOK, 16, 128),
        res,
        specialist_branch_scale.reshape(1, -1),
        specialist_switch_matrix[0],
        specialist_expand_matrix[0],
        specialist_contract_matrix[0],
    )
    return out[None]


def solution(mesh):
    return jax.shard_map(
        shards,
        mesh=mesh,
        in_specs=(
            P("dp", "sp", None),
            P("dp", "sp", None),
            P("dp", "sp", None),
            P("dp", "sp", None),
            P("dp", "sp", None),
            P("dp", "sp", None),
            P(),
            P(None, "dp"),
            P(),
            P(),
            P(("sp", "dp"), None, None),
            P(("sp", "dp"), None, None),
            P(("sp", "dp"), None, None),
            P(),
            P("dp", "sp", None),
            P("dp", "sp", None),
        ),
        out_specs=P("dp", "sp", None),
        check_vma=False,
    )
```

time: 300 us -> 140 us (0.47)
  Pallas kernels: 0 us -> 133 us
  waiting for transfers between devices: 81.2 us -> 0 us
  local copies, waits for them, and re-layouts: 84.8 us -> 4.76 us
  blocking collectives: 38.3 us -> 0 us
  other arithmetic: 36.5 us -> 2.41 us
  matrix products: 26.5 us -> 0.13 us
  starting transfers between devices: 17.1 us -> 0 us
  between operations: 14.1 us -> 0.06 us
    pallas_call x0 -> x2, Pallas kernels: none -> 133 us  [the longest x1 75.7 us: mixer(): pl.pallas_call(mixer_kernel, out_shape=(jax.ShapeDtypeStruct((TOK, D), bf...]
    all_to_all x3 -> x0, waiting for transfers between devices: 80.5 us -> none  [the longest x1 37.6 us: sent_together(): lax.all_to_all(both, axis, split_axis=split_dim, concat_axis=concat_dim,...]
    all_to_all x1 -> x0, blocking collectives: 38.3 us -> none  [one_exchange(): lax.all_to_all(pieces, axis, split_axis=0, concat_axis=0, tiled=True)]
    dot_general x6 -> x1, matrix products: 26.5 us -> 0.13 us  [routing(): rank = jnp.dot(before, named.astype(bf16), preferred_element_type=f32)]
    pad x6 -> x0, local copies, waits for them, and re-layouts: 23.8 us -> none  [block_attention(): lax.associative_scan(combine_states, (decays, updates), axis=0)]
    unnamed x56 -> x2, local copies, waits for them, and re-layouts: 20.9 us -> 2.67 us
    another operation x12 -> x0, local copies, waits for them, and re-layouts: 17.8 us -> none  [the longest x2 9.16 us: one_exchange(): pieces = pieces.reshape(-1, *inside)]
    add x13 -> x2, other arithmetic: 18 us -> 0.72 us  [the longest x1 0.71 us: routing(): (edp % 2 - c + 2) % 2 * 64 + (esp // 4 - z + 4) % 4 * 16]
  transfers between devices with their start and end apart: 4 -> 0, of which waited for: 3 -> 0; matrix products, arithmetic and copies ran while one was open for 30% -> 0% of each run, Pallas kernels for 0% -> 0%
where the time goes in v1:
time: 140 us
  Pallas kernels  133 us (95%)
  local copies, waits for them, and re-layouts  4.76 us (3%)
  other arithmetic  2.41 us (2%)
    pallas_call x1, Pallas kernels, mixer(): pl.pallas_call(mixer_kernel, out_shape=(jax.ShapeDtypeStruct((TOK, D), bf...  75.7 us
    pallas_call x1, Pallas kernels, experts(): pl.pallas_call(expert_kernel, out_shape=jax.ShapeDtypeStruct((TOK, D), bf...  56.9 us

profile of v1, /device:TPU:1, one launch (start us, length us, event | category | flops | bytes accessed | tf_op | source)
XLA Modules:
  0.0 140.0 jit_solution(12284143027639209125)
XLA Ops:
  0.0 0.7 fusion.4
  0.7 0.7 reduce_sum.29
  1.4 0.1 div.70
  1.5 0.1 div.71
  1.6 0.8 copy.22
  2.4 0.1 squeeze.36
  2.6 0.6 div.72.wts
  3.2 0.1 fusion
  3.3 0.1 broadcast_add_fusion
  3.4 0.1 multiply_reduce_fusion
  3.5 0.2 select_reduce_fusion
  3.7 0.1 copy.20
  3.8 0.8 convert_element_type.40.tab
  4.6 0.1 copy.21
  4.8 0.7 convert_element_type.42.slots
  5.5 75.7 %mixer.1 = (bf16[128,2048]{1,0:T(8,128)(2,1)}, bf16[2048,128]{1,0:T(8,128)(2,1)}) custom-call(bf16[128,2048]{1,0:T(8,128)(2,1)} %bitcast.37, bf16[128,2048]{1,0:T(8,128)(2,1)} %bitcast.38, bf16[128,2048]{1,0:T(8,128)(2,1)} %bitcast.39, bf16[128,4096]{1,0:T(8,128)(2,1)} %bitcast.35, bf16[128,2048]{1,0:T(8,128)(2,1)} %bitcast.40, f32[1,2048]{1,0:T(1,128)} %bitcast.43, ...), custom_call_target="tpu_custom_call" | custom-call | tf_op jit(solution)/shard_map/mixer/pallas_call | solution.py:282
  81.2 56.9 %experts.1 = bf16[128,2048]{1,0:T(8,128)(2,1)} custom-call(s32[384]{0:T(512)} %convert_element_type.40.tab, s32[256]{0:T(256)} %convert_element_type.42.slots, f32[256]{0:T(256)} %div.72.wts, bf16[128,16,128]{2,1,0:T(8,128)(2,1)} %bitcast.36, bf16[128,2048]{1,0:T(8,128)(2,1)} %get-tuple-element.8.res, f32[1,2048]{1,0:T(1,128)} %bitcast.42, ...), custom_call_target="tpu_custom_call" | custom-call | tf_op jit(solution)/shard_map/experts/pallas_call | solution.py:456
  138.1 1.9 %copy.24 = bf16[1,128,2048]{2,1,0:T(8,128)(2,1)} copy(bf16[1,128,2048]{2,1,0:T(8,128)(2,1)} %bitcast.34) | data formatting | bytes 1048576
  (5 shorter events, 0.0 us)

commit v2 on v1

v2 whole, which is shorter than its diff:
```python
import jax
import jax.numpy as jnp
from jax import lax
from jax.experimental import pallas as pl
from jax.experimental.pallas import tpu as pltpu
from jax.sharding import PartitionSpec as P

MESH = pl.DeviceIdType.MESH
D = 2048
HEADS = 16
KW = 128
DV = 256
FF = 1024
TOK = 128
TOP = 2
CAP = 3
EXPERTS = 128
PIECE = 512
HALF = 64
GROUPS = 2
PER = EXPERTS // GROUPS

epsilon = 1e-06
f32 = jnp.float32
bf16 = jnp.bfloat16


def dot_t(a, b, ca, cb):
    return lax.dot_general(a, b, (((ca,), (cb,)), ((), ())), preferred_element_type=f32)


def phases():
    held = []

    def begin(name):
        if held:
            held.pop().__exit__(None, None, None)
        if name:
            scope = jax.named_scope(name)
            scope.__enter__()
            held.append(scope)

    return begin


def layer_kernel(
    q_h, k_h, g_h, v_h, skip_h, spk, w_h, gs, bg, pg, chosen, logits, gain, wg_h, wu_h, wd_h,
    res_out, norm_out,
    qv, kv, gv, vv, skipv, spk_in, wall,
    bgs, lf, lw, ca, lt, intra, us, ur, dsend, drecv, ss, sr, tall, pj, po, rf,
    x3, xs, xr, ys, yr, xm, hs, wg, wu, wd, idx_v, wts_v, idx, wts,
    lsem, spk_s, spk_r, w_s, w_r, u_s, u_r, d_s, d_r, s_s, s_r, t_s, t_r, p_s, p_r,
    esem, isem, x_s, x_r, y_s, y_r,
):
    ph = phases()
    sp = lax.axis_index("sp")
    dp = lax.axis_index("dp")
    z, x = sp // 4, sp % 4
    y, c = dp // 2, dp % 2
    partner = (sp, y * 2 + (1 - c))
    dps = [[((y + dy) % 4) * 2 + (c + dc) % 2 for dc in range(2)] for dy in range(4)]

    def ahead(i):
        return ((z + i // 4) % 4) * 4 + (x + i % 4) % 4

    def behind(i):
        return ((z + 4 - i // 4) % 4) * 4 + (x + 4 - i % 4) % 4

    def remote(src, dst, s, r, dev):
        return pltpu.make_async_remote_copy(
            src_ref=src, dst_ref=dst, send_sem=s, recv_sem=r, device_id=dev, device_id_type=MESH
        )

    ph("m_start")
    loads = [
        pltpu.make_async_copy(g_h, gv, lsem.at[0]),
        pltpu.make_async_copy(k_h, kv, lsem.at[1]),
        pltpu.make_async_copy(v_h, vv, lsem.at[2]),
        pltpu.make_async_copy(q_h, qv, lsem.at[3]),
        pltpu.make_async_copy(skip_h, skipv, lsem.at[4]),
        pltpu.make_async_copy(w_h, wall.at[0], lsem.at[5]),
    ]
    for one in loads:
        one.start()

    barrier = pltpu.get_barrier_semaphore()

    def greet(to, skip):
        for dy in range(4):
            for dc in range(2):
                if not (skip and dy == 0 and dc == 0):
                    pl.semaphore_signal(
                        barrier, inc=1, device_id=(to, dps[dy][dc]), device_id_type=MESH
                    )

    greet(sp, True)

    @pl.loop(1, HEADS)
    def _(i):
        greet(ahead(i), False)

    row = lax.broadcasted_iota(jnp.int32, (TOK, TOK), 0)
    col = lax.broadcasted_iota(jnp.int32, (TOK, TOK), 1)
    same = (row >= col) & ((row >= HALF) == (col >= HALF))
    cross = (row >= HALF) & (col < HALF)
    first = row < HALF
    tri = jnp.where(same, 1.0, 0.0).astype(bf16)

    def split(a):
        hi = a.astype(bf16)
        rest = a - hi.astype(f32)
        mid = rest.astype(bf16)
        return hi, mid, (rest - mid.astype(f32)).astype(bf16)

    ph("m_decay")
    loads[0].wait()

    @pl.loop(0, HEADS // 2)
    def _(i):
        for k in range(2):
            h = i * 2 + k
            g = gv[:, pl.ds(pl.multiple_of(h * KW, KW), KW)].astype(f32)
            ld = (jnp.minimum(g, 0.0) - jnp.log1p(jnp.exp(-jnp.abs(g)))) * (1.0 / 16.0)
            hi, mid, low = split(ld)
            bgs[h] = dot_t(tri, hi, 1, 0) + dot_t(tri, mid, 1, 0) + dot_t(tri, low, 1, 0)

    ph("m_barrier")
    pl.semaphore_wait(barrier, EXPERTS - 1)
    ph("m_first")
    pltpu.make_async_copy(
        spk.at[:, pl.ds(pl.multiple_of(sp * TOK, TOK), TOK)], spk_in.at[sp], spk_r
    ).start()

    @pl.loop(1, HEADS)
    def _(i):
        to = (sp + i) % HEADS
        remote(
            spk.at[:, pl.ds(pl.multiple_of(to * TOK, TOK), TOK)], spk_in.at[sp], spk_s, spk_r, (to, dp)
        ).start()

    base = ((x + z) % 2) * 4
    obase = 4 - base
    up = (sp, dps[1][0])
    down = (sp, dps[3][0])
    around = [(ahead(1), dp), (ahead(3), dp), (ahead(4), dp), (ahead(12), dp)]

    def rows(piece):
        return pl.ds(pl.multiple_of(piece * PIECE, PIECE), PIECE)

    for i in range(4):
        a, b = base + i, base + (i + 2) % 4
        remote(w_h.at[rows(a)], wall.at[1, rows(a)], w_s, w_r.at[0, a], up).start()
        remote(w_h.at[rows(b)], wall.at[3, rows(b)], w_s, w_r.at[2, b], down).start()

    def w_wait(slot, piece):
        there = wall.at[slot, rows(piece)]
        remote(there, there, w_s, w_r.at[slot - 1, piece], partner).wait_recv()

    def w_pass(slot, i):
        piece = base + i
        w_wait(slot, piece)
        there = wall.at[slot, rows(piece)]
        if slot == 1 and i < 2:
            remote(there, wall.at[2, rows(piece)], w_s, w_r.at[1, piece], up).start()
        if slot == 3 and i >= 2:
            remote(there, wall.at[2, rows(piece)], w_s, w_r.at[1, piece], down).start()
        remote(there, there, w_s, w_r.at[slot - 1, piece], around[i]).start()

    ph("m_route")
    esp, edp = chosen[...] >> 3, chosen[...] & 7
    off = (
        (((edp & 1) + c) & 1) * 64
        + (((esp >> 2) + 4 - z) & 3) * 16
        + (((esp & 3) + 4 - x) & 3) * 4
        + (((edp >> 1) + 4 - y) & 3)
    )
    pick = [jnp.where(row == off[r : r + 1], 1.0, 0.0) for r in range(TOP)]
    named = pick[0] + pick[1]
    later = jnp.where(row < col, 1.0, 0.0).astype(bf16)
    rank = dot_t(named.astype(bf16), later, 1, 0)
    place = row.astype(f32) * CAP + rank
    idx_v[...] = jnp.zeros((8, TOK), jnp.int32)
    times = jnp.where(lax.broadcasted_iota(jnp.int32, (8, TOK), 0) >= 0, 1.0, 0.0) * (
        lax.broadcasted_iota(jnp.int32, (8, TOK), 1).astype(f32)
    )
    for k in range(CAP):
        filled = jnp.where(rank == float(k), named, 0.0).astype(bf16)
        found = dot_t(times.astype(bf16), filled, 1, 1)
        idx_v[k : k + 1, :] = jnp.minimum(found[:1], TOK - 1.0).astype(jnp.int32)
    for r in range(TOP):
        at = jnp.sum(pick[r] * place, axis=0, keepdims=True)
        idx_v[CAP + r : CAP + r + 1, :] = jnp.minimum(at, EXPERTS * CAP - 1.0).astype(jnp.int32)
    lg = logits[...]
    wts_v[...] = lg / (lg[0:1] + lg[1:2])
    tables = [
        pltpu.make_async_copy(idx_v, idx, isem.at[0]),
        pltpu.make_async_copy(wts_v, wts, isem.at[1]),
    ]

    ph("m_loadwait")
    for one in loads[1:4]:
        one.wait()
    remote(spk_in.at[pl.ds(0, HEADS)], spk_in.at[pl.ds(0, HEADS)], spk_s, spk_r, partner).wait_recv()
    ph("m_loopA")

    def u_send(h, part):
        rows_u = pl.ds(part * TOK, TOK)
        remote(us.at[h, rows_u], ur.at[sp, rows_u], u_s, u_r.at[part, sp], (h, dp)).start()

    def form(h):
        lanes = pl.ds(pl.multiple_of(h * KW, KW), KW)
        hi, mid, low = split(jnp.broadcast_to(spk_in[h], (TOK, TOK)).T)
        b = bgs[h] + dot_t(tri, hi, 1, 0) + dot_t(tri, mid, 1, 0) + dot_t(tri, low, 1, 0)
        e1, e2 = b[HALF - 1 : HALF, :], b[TOK - 1 : TOK, :]
        kf = kv[:, lanes].astype(f32)
        qf = qv[:, lanes].astype(f32) * KW ** (-0.5)
        carried = kf * jnp.exp(jnp.where(first, e1, e2) - b)
        ku = carried * jnp.where(first, jnp.exp(e2), 1.0)
        vh = vv[:, pl.ds(pl.multiple_of(h * DV, DV), DV)]
        us[h] = dot_t(vh, ku.astype(bf16), 0, 0).astype(bf16)
        dsend[h] = jnp.exp(e1 + e2)
        lifted = qf * jnp.exp(b)
        lf[h] = lifted.astype(bf16)
        lw[h] = (kf * jnp.exp(-b)).astype(bf16)
        ca[h] = carried.astype(bf16)
        lt[h] = (lifted * jnp.where(first, 1.0, jnp.exp(e1))).astype(bf16)

    @pl.loop(0, HEADS // 2)
    def _(i):
        for k in range(2):
            form((sp + 1 + 2 * i + k) % HEADS)

        u_send((sp + 1 + 2 * i) % HEADS, 0)

        @pl.when(i < HEADS // 2 - 1)
        def _():
            u_send((sp + 2 + 2 * i) % HEADS, 0)

    ph("m_sendB")
    for part in range(2):
        rows_u = pl.ds(part * TOK, TOK)
        pltpu.make_async_copy(us.at[sp, rows_u], ur.at[sp, rows_u], u_r.at[part, sp]).start()
    pltpu.make_async_copy(dsend.at[sp], drecv.at[sp], d_r).start()

    @pl.loop(1, HEADS)
    def _(i):
        h = (sp + i) % HEADS
        remote(dsend.at[h], drecv.at[sp], d_s, d_r, (h, dp)).start()

    @pl.loop(1, HEADS)
    def _(i):
        u_send((sp + i) % HEADS, 1)

    for one in tables:
        one.start()
    experts_in = [
        pltpu.make_async_copy(wg_h, wg, esem.at[0]),
        pltpu.make_async_copy(wu_h, wu, esem.at[1]),
        pltpu.make_async_copy(wd_h, wd, esem.at[2]),
    ]
    for one in experts_in:
        one.start()

    ph("m_loopB")

    @pl.loop(0, HEADS // 2)
    def _(i):
        for k in range(2):
            h = 2 * i + k
            vh = vv[:, pl.ds(pl.multiple_of(h * DV, DV), DV)]
            near = dot_t(lf[h], lw[h], 1, 1)
            far = dot_t(lf[h], ca[h], 1, 1)
            scores = jnp.where(same, near, jnp.where(cross, far, 0.0))
            intra[h] = dot_t(scores.astype(bf16), vh, 1, 0)

    ph("m_w0")
    w_pass(1, 0)
    w_pass(3, 2)
    ph("m_dwait")
    remote(drecv.at[pl.ds(0, HEADS)], drecv.at[pl.ds(0, HEADS)], d_s, d_r, partner).wait_recv()

    for part in range(2):
        ph(f"m_scan{part}")
        rows_u = pl.ds(part * TOK, TOK)

        def step(src, state, rows_u=rows_u, part=part):
            ss[src, rows_u] = state.astype(bf16)

            @pl.when(src != sp)
            def _():
                remote(ss.at[src, rows_u], sr.at[sp, rows_u], s_s, s_r.at[part, sp], (src, dp)).start()

            @pl.when(src == sp)
            def _():
                pltpu.make_async_copy(ss.at[sp, rows_u], sr.at[sp, rows_u], s_r.at[part, sp]).start()

            there = ur.at[src, rows_u]
            remote(there, there, u_s, u_r.at[part, src], partner).wait_recv()
            return state * drecv[src] + ur[src, rows_u].astype(f32)

        lax.fori_loop(0, HEADS, step, jnp.zeros((TOK, KW), f32))
        ph(f"m_w{part + 1}")
        w_pass(1, part + 1)
        w_pass(3, (part + 3) % 4)

    def attend(i):
        h = (sp + i) % HEADS
        for part in range(2):
            there = sr.at[h, pl.ds(part * TOK, TOK)]
            remote(there, there, s_s, s_r.at[part, h], partner).wait_recv()
        o = intra[h] + dot_t(lt[h], sr[h], 1, 1)
        ms = jnp.mean(o * o, axis=-1, keepdims=True)
        lanes = pl.ds(pl.multiple_of(h * DV, DV), DV)
        tall[pl.ds(0, TOK), lanes] = (o * lax.rsqrt(ms + epsilon) * gs[:, lanes]).astype(bf16)

    def t_send(i):
        lanes = pl.ds(pl.multiple_of(((sp + i) % HEADS) * DV, DV), DV)
        remote(tall.at[pl.ds(0, TOK), lanes], tall.at[pl.ds(TOK, TOK), lanes], t_s, t_r, partner).start()

    ph("m_w3")
    w_pass(1, 3)
    w_pass(3, 1)
    for part in range(2):
        ph(f"m_loopC{part}")

        @pl.loop(part * 4, part * 4 + 4)
        def _(i):
            attend(2 * i)

            @pl.when(i > 0)
            def _():
                t_send(2 * i - 1)

            attend(2 * i + 1)
            t_send(2 * i)

        ph(f"m_w{part + 4}")
        w_pass(2, part)
        w_pass(2, part + 2)

    ph("m_twait")
    t_send(HEADS - 1)
    loads[4].wait()
    loads[5].wait()
    remote(tall.at[pl.ds(0, TOK)], tall.at[pl.ds(TOK, TOK)], t_s, t_r, partner).wait_recv()

    def project(slot):
        acc = jnp.dot(tall[...], wall[slot], preferred_element_type=f32).astype(bf16)
        shard = ((y + 4 - slot) % 4) * 2 + c
        po[slot] = acc[TOK:]
        pj[shard] = acc[:TOK]
        remote(po.at[slot], pj.at[shard], p_s, p_r, partner).start()

    ph("m_proj0")
    project(0)
    for slot in (1, 3, 2):
        ph(f"m_ow{slot}")
        for i in range(4):
            w_wait(slot, obase + i)
        ph(f"m_proj{slot}")
        project(slot)
    ph("m_pwait")
    remote(po.at[pl.ds(0, 4)], pj.at[pl.ds(0, 4)], p_s, p_r, partner).wait_recv()

    ph("m_norm")
    total = jnp.zeros((TOK, 1), f32)
    for n in range(8):
        p = pj[n].astype(f32)
        total = total + jnp.sum(p * p, axis=-1, keepdims=True)
    r1 = lax.rsqrt(total * (1.0 / D) + epsilon)
    total = jnp.zeros((TOK, 1), f32)
    for n in range(8):
        lanes = pl.ds(n * 256, 256)
        res = (skipv[:, lanes].astype(f32) + pj[n].astype(f32) * r1 * bg[:, lanes]).astype(bf16)
        res_out[:, lanes] = res
        rs = res.astype(f32)
        total = total + jnp.sum(rs * rs, axis=-1, keepdims=True)
    r2 = lax.rsqrt(total * (1.0 / D) + epsilon)
    for j in range(16):
        lanes = pl.ds(j * 128, 128)
        rf[pl.ds(j, TOK, stride=16), :] = res_out[:, lanes].astype(f32) * r2 * pg[:, lanes]

    @pl.loop(0, 8)
    def _(i):
        x3[pl.ds(i * 16, 16)] = (
            rf[pl.ds(pl.multiple_of(i * 256, 256), 256), :].reshape(16, 16, 128).astype(bf16)
        )

    ph("e_pack")
    for one in tables:
        one.wait()

    def pack(grp):
        @pl.loop(0, PER // 4)
        def _(i):
            for u in range(4):
                o = grp * PER + i * 4 + u
                for k in range(CAP):
                    xs[o * CAP + k] = x3[jnp.clip(idx[k, o], 0, TOK - 1)]

    def send(grp, src, dst, s, r, place_of, sign):
        def one(i, to, dy):
            at = pl.ds((grp * PER + i * 4 + dy) * CAP, CAP)
            remote(src.at[at], dst.at[at], s, r.at[grp], (to, dps[(sign * dy) % 4][grp])).start()

        if grp == 0:
            pltpu.make_async_copy(src.at[pl.ds(0, CAP)], dst.at[pl.ds(0, CAP)], r.at[0]).start()

        @pl.loop(0, HEADS if grp else HEADS - 1)
        def _(j):
            i = HEADS - 1 - j
            to = place_of(i)
            for dy in (3, 2, 1, 0):
                one(i, to, dy)

        if grp == 0:
            for dy in (3, 2, 1):
                one(0, sp, dy)

    for grp in range(GROUPS):
        pack(grp)
        send(grp, xs, xr, x_s, x_r, ahead, 1)

    R = PER * CAP
    for grp in range(GROUPS):
        ph(f"e_xwait{grp}")
        at = pl.ds(grp * R, R)
        remote(xr.at[at], xr.at[at], x_s, x_r.at[grp], partner).wait_recv()
        ph(f"e_relay{grp}")

        @pl.loop(0, R // 12)
        def _(i):
            rf[pl.ds(pl.multiple_of(i * 192, 192), 192), :] = (
                xr[pl.ds(grp * R + i * 12, 12)].astype(f32).reshape(192, 128)
            )

        for j in range(16):
            xm[:, pl.ds(j * 128, 128)] = rf[pl.ds(j, R, stride=16), :].astype(bf16)
        ph(f"e_mlp{grp}")
        if grp == 0:
            experts_in[0].wait()
            experts_in[1].wait()

        @pl.loop(0, FF // 256)
        def _(n):
            lanes = pl.ds(pl.multiple_of(n * 256, 256), 256)
            a = jnp.dot(xm[...], wg[:, lanes], preferred_element_type=f32)
            b = jnp.dot(xm[...], wu[:, lanes], preferred_element_type=f32)
            hs[:, lanes] = (a * (1.0 / (1.0 + jnp.exp(-a))) * b).astype(bf16)

        if grp == 0:
            experts_in[2].wait()

        @pl.loop(0, D // 256)
        def _(n):
            lanes = pl.ds(pl.multiple_of(n * 256, 256), 256)
            a = jnp.dot(hs[...], wd[:, lanes], preferred_element_type=f32)
            rf[pl.ds(2 * n, R, stride=16), :] = a[:, :128]
            rf[pl.ds(2 * n + 1, R, stride=16), :] = a[:, 128:]

        ph(f"e_yrelay{grp}")

        @pl.loop(0, R // 12)
        def _(i):
            ys[pl.ds(grp * R + i * 12, 12)] = (
                rf[pl.ds(pl.multiple_of(i * 192, 192), 192), :].reshape(12, 16, 128).astype(bf16)
            )

        ph(f"e_ysend{grp}")
        send(grp, ys, yr, y_s, y_r, behind, -1)

    for grp in range(GROUPS):
        ph(f"e_ywait{grp}")
        at = pl.ds(grp * R, R)
        remote(yr.at[at], yr.at[at], y_s, y_r.at[grp], partner).wait_recv()

    ph("e_comb")

    @pl.loop(0, TOK // 4)
    def _(i):
        for k in range(4):
            t = i * 4 + k
            one = yr[jnp.clip(idx[CAP, t], 0, EXPERTS * CAP - 1)].astype(f32) * wts[0, t]
            two = yr[jnp.clip(idx[CAP + 1, t], 0, EXPERTS * CAP - 1)].astype(f32) * wts[1, t]
            rf[pl.ds(pl.multiple_of(t * 16, 16), 16), :] = one + two

    ph("e_norm")
    total = jnp.zeros((TOK, 1), f32)
    for j in range(16):
        p = rf[pl.ds(j, TOK, stride=16), :]
        total = total + jnp.sum(p * p, axis=-1, keepdims=True)
    r1 = lax.rsqrt(total * (1.0 / D) + epsilon)
    for j in range(16):
        lanes = pl.ds(j * 128, 128)
        norm_out[:, lanes] = rf[pl.ds(j, TOK, stride=16), :] * r1 * gain[:, lanes]

    ph("e_sendwait")
    fifteen = pl.ds(0, HEADS - 1)
    most = pl.ds(0, (EXPERTS - 1) * CAP)
    remote(spk_in.at[fifteen], spk_in.at[fifteen], spk_s, spk_r, partner).wait_send()
    remote(drecv.at[fifteen], drecv.at[fifteen], d_s, d_r, partner).wait_send()
    remote(us.at[fifteen], ur.at[fifteen], u_s, u_r.at[0, 0], partner).wait_send()
    remote(ss.at[fifteen], sr.at[fifteen], s_s, s_r.at[0, 0], partner).wait_send()
    remote(tall.at[pl.ds(0, TOK)], tall.at[pl.ds(TOK, TOK)], t_s, t_r, partner).wait_send()
    remote(po.at[pl.ds(0, 4)], pj.at[pl.ds(0, 4)], p_s, p_r, partner).wait_send()
    remote(wall.at[pl.ds(0, 3)], wall.at[pl.ds(0, 3)], w_s, w_r.at[0, 0], partner).wait_send()
    remote(xs.at[most], xr.at[most], x_s, x_r.at[0], partner).wait_send()
    remote(ys.at[most], yr.at[most], y_s, y_r.at[0], partner).wait_send()
    ph(None)


def layer(*args):
    hbm = pl.BlockSpec(memory_space=pl.ANY)
    vmem = pl.BlockSpec(memory_space=pltpu.VMEM)
    dma = pltpu.SemaphoreType.DMA
    R = PER * CAP
    return pl.pallas_call(
        layer_kernel,
        out_shape=(
            jax.ShapeDtypeStruct((TOK, D), bf16),
            jax.ShapeDtypeStruct((TOK, D), f32),
        ),
        in_specs=[hbm] * 5 + [vmem, hbm] + [vmem] * 6 + [hbm] * 3,
        out_specs=(vmem, vmem),
        scratch_shapes=[
            pltpu.VMEM((TOK, D), bf16),
            pltpu.VMEM((TOK, D), bf16),
            pltpu.VMEM((TOK, D), bf16),
            pltpu.VMEM((TOK, HEADS * DV), bf16),
            pltpu.VMEM((TOK, D), bf16),
            pltpu.VMEM((HEADS, 1, TOK), f32),
            pltpu.VMEM((4, HEADS * DV, 256), bf16),
            pltpu.VMEM((HEADS, TOK, KW), f32),
            pltpu.VMEM((HEADS, TOK, KW), bf16),
            pltpu.VMEM((HEADS, TOK, KW), bf16),
            pltpu.VMEM((HEADS, TOK, KW), bf16),
            pltpu.VMEM((HEADS, TOK, KW), bf16),
            pltpu.VMEM((HEADS, TOK, DV), f32),
            pltpu.VMEM((HEADS, DV, KW), bf16),
            pltpu.VMEM((HEADS, DV, KW), bf16),
            pltpu.VMEM((HEADS, 1, KW), f32),
            pltpu.VMEM((HEADS, 1, KW), f32),
            pltpu.VMEM((HEADS, DV, KW), bf16),
            pltpu.VMEM((HEADS, DV, KW), bf16),
            pltpu.VMEM((2 * TOK, HEADS * DV), bf16),
            pltpu.VMEM((8, TOK, 256), bf16),
            pltpu.VMEM((4, TOK, 256), bf16),
            pltpu.VMEM((R * 16, 128), f32),
            pltpu.VMEM((TOK, 16, 128), bf16),
            pltpu.VMEM((EXPERTS * CAP, 16, 128), bf16),
            pltpu.VMEM((EXPERTS * CAP, 16, 128), bf16),
            pltpu.VMEM((EXPERTS * CAP, 16, 128), bf16),
            pltpu.VMEM((EXPERTS * CAP, 16, 128), bf16),
            pltpu.VMEM((R, D), bf16),
            pltpu.VMEM((R, FF), bf16),
            pltpu.VMEM((D, FF), bf16),
            pltpu.VMEM((D, FF), bf16),
            pltpu.VMEM((FF, D), bf16),
            pltpu.VMEM((8, TOK), jnp.int32),
            pltpu.VMEM((TOP, TOK), f32),
            pltpu.SMEM((8, TOK), jnp.int32),
            pltpu.SMEM((TOP, TOK), f32),
            dma((6,)),
            dma, dma,
            dma, dma((3, 8)),
            dma, dma((2, HEADS)),
            dma, dma,
            dma, dma((2, HEADS)),
            dma, dma,
            dma, dma,
            dma((3,)), dma((2,)),
            dma, dma((GROUPS,)),
            dma, dma((GROUPS,)),
        ],
        compiler_params=pltpu.CompilerParams(
            collective_id=0, has_side_effects=True, vmem_limit_bytes=58 * 2**20
        ),
        name="layer",
    )(*args)


def shards(
    skip_stream_entering,
    mapped_probe_matrix,
    mapped_lookup_matrix,
    mapped_content_matrix,
    retention_preactivation,
    extra_shrinkage,
    attention_group_scale,
    final_projection_matrix,
    blender_branch_scale,
    specialist_prenormal_scale,
    specialist_switch_matrix,
    specialist_expand_matrix,
    specialist_contract_matrix,
    specialist_branch_scale,
    assigned_specialists,
    dispatcher_logits,
):
    res, norm = layer(
        mapped_probe_matrix[0],
        mapped_lookup_matrix[0],
        retention_preactivation[0],
        mapped_content_matrix[0],
        skip_stream_entering[0],
        extra_shrinkage[0],
        final_projection_matrix,
        attention_group_scale.reshape(1, -1),
        blender_branch_scale.reshape(1, -1),
        specialist_prenormal_scale.reshape(1, -1),
        assigned_specialists[0].T,
        dispatcher_logits[0].T,
        specialist_branch_scale.reshape(1, -1),
        specialist_switch_matrix[0],
        specialist_expand_matrix[0],
        specialist_contract_matrix[0],
    )
    return (res.astype(f32) + norm).astype(bf16)[None]


def solution(mesh):
    return jax.shard_map(
        shards,
        mesh=mesh,
        in_specs=(
            P("dp", "sp", None),
            P("dp", "sp", None),
            P("dp", "sp", None),
            P("dp", "sp", None),
            P("dp", "sp", None),
            P("dp", "sp", None),
            P(),
            P(None, "dp"),
            P(),
            P(),
            P(("sp", "dp"), None, None),
            P(("sp", "dp"), None, None),
            P(("sp", "dp"), None, None),
            P(),
            P("dp", "sp", None),
            P("dp", "sp", None),
        ),
        out_specs=P("dp", "sp", None),
        check_vma=False,
    )
```

time: 140 us -> 116 us (0.83)
  Pallas kernels: 133 us -> 113 us
  local copies, waits for them, and re-layouts: 4.76 us -> 0 us
    pallas_call x2 -> x1, Pallas kernels: 133 us -> 113 us  [layer(): pl.pallas_call(layer_kernel, out_shape=(jax.ShapeDtypeStruct((TOK, D), bf...]
    unnamed x2 -> x0, local copies, waits for them, and re-layouts: 2.67 us -> none
    broadcast_in_dim x0 -> x1, other arithmetic: none -> 2.26 us  [shards(): return (res.astype(f32) + norm).astype(bf16)[None]]
    convert_element_type x4 -> x0, local copies, waits for them, and re-layouts: 1.73 us -> none  [the longest x2 0.9 us: routing(): jnp.sum(filled * time.astype(f32)[:, None, None], axis=0).astype(jnp.int32)]
where the time goes in v2:
time: 116 us; the launch traced here: 115 us
  Pallas kernels  113 us (97%)
  other arithmetic  2.26 us (2%)
    pallas_call x1, Pallas kernels, layer(): pl.pallas_call(layer_kernel, out_shape=(jax.ShapeDtypeStruct((TOK, D), bf...  113 us

profile of v2, /device:TPU:1, one launch (start us, length us, event | category | flops | bytes accessed | tf_op | source)
XLA Modules:
  0.0 115.1 jit_solution(18030511286723122246)
XLA Ops:
  0.0 112.8 %layer.1 = (bf16[128,2048]{1,0:T(8,128)(2,1)}, f32[128,2048]{1,0:T(8,128)}) custom-call(bf16[128,2048]{1,0:T(8,128)(2,1)} %bitcast.25, bf16[128,2048]{1,0:T(8,128)(2,1)} %bitcast.26, bf16[128,2048]{1,0:T(8,128)(2,1)} %bitcast.27, bf16[128,4096]{1,0:T(8,128)(2,1)} %bitcast.24, bf16[128,2048]{1,0:T(8,128)(2,1)} %bitcast.28, f32[1,2048]{1,0:T(1,128)} %bitcast.30, ...), custom_call_target="tpu_custom_call" | custom-call | tf_op jit(solution)/shard_map/layer/pallas_call | solution.py:517
  112.8 2.3 %fusion = bf16[1,128,2048]{2,1,0:T(8,128)(2,1)} fusion(f32[128,2048]{1,0:T(8,128)} %get-tuple-element.8, bf16[128,2048]{1,0:T(8,128)(2,1)} %get-tuple-element.7), kind=kLoop, calls=%fused_computation.1 | loop fusion | flops 786432 | bytes 2097152 | tf_op jit(solution)/shard_map/broadcast_in_dim | solution.py:618

commit v3 on v2

--- a/solution.py
+++ b/solution.py
@@ -17,7 +17,7 @@
 EXPERTS = 128
 PIECE = 512
 HALF = 64
-GROUPS = 2
+GROUPS = 4
 PER = EXPERTS // GROUPS
 
 epsilon = 1e-06
@@ -45,11 +45,11 @@
 
 def layer_kernel(
     q_h, k_h, g_h, v_h, skip_h, spk, w_h, gs, bg, pg, chosen, logits, gain, wg_h, wu_h, wd_h,
-    res_out, norm_out,
-    qv, kv, gv, vv, skipv, spk_in, wall,
+    out,
+    res_v, qv, kv, gv, vv, skipv, spk_in, wall,
     bgs, lf, lw, ca, lt, intra, us, ur, dsend, drecv, ss, sr, tall, pj, po, rf,
     x3, xs, xr, ys, yr, xm, hs, wg, wu, wd, idx_v, wts_v, idx, wts,
-    lsem, spk_s, spk_r, w_s, w_r, u_s, u_r, d_s, d_r, s_s, s_r, t_s, t_r, p_s, p_r,
+    ready, lsem, spk_s, spk_r, w_s, w_r, u_s, u_r, d_s, d_r, s_s, s_r, t_s, t_r, p_s, p_r,
     esem, isem, x_s, x_r, y_s, y_r,
 ):
     ph = phases()
@@ -62,9 +62,6 @@
 
     def ahead(i):
         return ((z + i // 4) % 4) * 4 + (x + i % 4) % 4
-
-    def behind(i):
-        return ((z + 4 - i // 4) % 4) * 4 + (x + 4 - i % 4) % 4
 
     def remote(src, dst, s, r, dev):
         return pltpu.make_async_remote_copy(
@@ -85,19 +82,15 @@
 
     barrier = pltpu.get_barrier_semaphore()
 
-    def greet(to, skip):
-        for dy in range(4):
-            for dc in range(2):
-                if not (skip and dy == 0 and dc == 0):
-                    pl.semaphore_signal(
-                        barrier, inc=1, device_id=(to, dps[dy][dc]), device_id_type=MESH
-                    )
-
-    greet(sp, True)
+    mates = [dps[dy][dc] for dy in range(4) for dc in range(2)][1:]
+    for mate in mates:
+        pl.semaphore_signal(barrier, inc=1, device_id=(sp, mate), device_id_type=MESH)
 
     @pl.loop(1, HEADS)
     def _(i):
-        greet(ahead(i), False)
+        pl.semaphore_signal(
+            barrier, inc=1, device_id=((sp + i) % HEADS, dp), device_id_type=MESH
+        )
 
     row = lax.broadcasted_iota(jnp.int32, (TOK, TOK), 0)
     col = lax.broadcasted_iota(jnp.int32, (TOK, TOK), 1)
@@ -112,20 +105,10 @@
         mid = rest.astype(bf16)
         return hi, mid, (rest - mid.astype(f32)).astype(bf16)
 
-    ph("m_decay")
-    loads[0].wait()
-
-    @pl.loop(0, HEADS // 2)
-    def _(i):
-        for k in range(2):
-            h = i * 2 + k
-            g = gv[:, pl.ds(pl.multiple_of(h * KW, KW), KW)].astype(f32)
-            ld = (jnp.minimum(g, 0.0) - jnp.log1p(jnp.exp(-jnp.abs(g)))) * (1.0 / 16.0)
-            hi, mid, low = split(ld)
-            bgs[h] = dot_t(tri, hi, 1, 0) + dot_t(tri, mid, 1, 0) + dot_t(tri, low, 1, 0)
-
     ph("m_barrier")
-    pl.semaphore_wait(barrier, EXPERTS - 1)
+    pl.semaphore_wait(barrier, HEADS - 1 + len(mates))
+    for mate in mates:
+        pl.semaphore_signal(ready, inc=1, device_id=(sp, mate), device_id_type=MESH)
     ph("m_first")
     pltpu.make_async_copy(
         spk.at[:, pl.ds(pl.multiple_of(sp * TOK, TOK), TOK)], spk_in.at[sp], spk_r
@@ -166,13 +149,25 @@
             remote(there, wall.at[2, rows(piece)], w_s, w_r.at[1, piece], down).start()
         remote(there, there, w_s, w_r.at[slot - 1, piece], around[i]).start()
 
+    ph("m_decay")
+    loads[0].wait()
+
+    @pl.loop(0, HEADS // 2)
+    def _(i):
+        for k in range(2):
+            h = i * 2 + k
+            g = gv[:, pl.ds(pl.multiple_of(h * KW, KW), KW)].astype(f32)
+            ld = (jnp.minimum(g, 0.0) - jnp.log1p(jnp.exp(-jnp.abs(g)))) * (1.0 / 16.0)
+            hi, mid, low = split(ld)
+            bgs[h] = dot_t(tri, hi, 1, 0) + dot_t(tri, mid, 1, 0) + dot_t(tri, low, 1, 0)
+
     ph("m_route")
     esp, edp = chosen[...] >> 3, chosen[...] & 7
     off = (
-        (((edp & 1) + c) & 1) * 64
-        + (((esp >> 2) + 4 - z) & 3) * 16
-        + (((esp & 3) + 4 - x) & 3) * 4
-        + (((edp >> 1) + 4 - y) & 3)
+        (((esp & 3) - (esp >> 2) + 8 - x + z) & 3) * 32
+        + (((esp >> 2) + 4 - z) & 3) * 8
+        + (((edp >> 1) + 4 - y) & 3) * 2
+        + (((edp & 1) + c) & 1)
     )
     pick = [jnp.where(row == off[r : r + 1], 1.0, 0.0) for r in range(TOP)]
     named = pick[0] + pick[1]
@@ -204,8 +199,13 @@
     ph("m_loopA")
 
     def u_send(h, part):
-        rows_u = pl.ds(part * TOK, TOK)
-        remote(us.at[h, rows_u], ur.at[sp, rows_u], u_s, u_r.at[part, sp], (h, dp)).start()
+        if part == 0:
+            remote(dsend.at[h], drecv.at[sp], d_s, d_r, (h, dp)).start()
+
+        @pl.when(sp < HEADS - 1)
+        def _():
+            rows_u = pl.ds(part * TOK, TOK)
+            remote(us.at[h, rows_u], ur.at[sp, rows_u], u_s, u_r.at[part, sp], (h, dp)).start()
 
     def form(h):
         lanes = pl.ds(pl.multiple_of(h * KW, KW), KW)
@@ -237,15 +237,20 @@
             u_send((sp + 2 + 2 * i) % HEADS, 0)
 
     ph("m_sendB")
-    for part in range(2):
-        rows_u = pl.ds(part * TOK, TOK)
-        pltpu.make_async_copy(us.at[sp, rows_u], ur.at[sp, rows_u], u_r.at[part, sp]).start()
+
+    @pl.when(sp < HEADS - 1)
+    def _():
+        for part in range(2):
+            rows_u = pl.ds(part * TOK, TOK)
+            pltpu.make_async_copy(us.at[sp, rows_u], ur.at[sp, rows_u], u_r.at[part, sp]).start()
+
+    @pl.when(sp == 0)
+    def _():
+        @pl.loop(0, HEADS)
+        def _(i):
+            sr[i] = jnp.zeros((DV, KW), bf16)
+
     pltpu.make_async_copy(dsend.at[sp], drecv.at[sp], d_r).start()
-
-    @pl.loop(1, HEADS)
-    def _(i):
-        h = (sp + i) % HEADS
-        remote(dsend.at[h], drecv.at[sp], d_s, d_r, (h, dp)).start()
 
     @pl.loop(1, HEADS)
     def _(i):
@@ -284,30 +289,36 @@
         rows_u = pl.ds(part * TOK, TOK)
 
         def step(src, state, rows_u=rows_u, part=part):
-            ss[src, rows_u] = state.astype(bf16)
-
-            @pl.when(src != sp)
+            there = ur.at[src, rows_u]
+            remote(there, there, u_s, u_r.at[part, src], partner).wait_recv()
+            state = state * drecv[src] + ur[src, rows_u].astype(f32)
+            to = src + 1
+            ss[to, rows_u] = state.astype(bf16)
+
+            @pl.when(to != sp)
             def _():
-                remote(ss.at[src, rows_u], sr.at[sp, rows_u], s_s, s_r.at[part, sp], (src, dp)).start()
-
-            @pl.when(src == sp)
+                remote(ss.at[to, rows_u], sr.at[sp, rows_u], s_s, s_r.at[part, sp], (to, dp)).start()
+
+            @pl.when(to == sp)
             def _():
                 pltpu.make_async_copy(ss.at[sp, rows_u], sr.at[sp, rows_u], s_r.at[part, sp]).start()
 
-            there = ur.at[src, rows_u]
-            remote(there, there, u_s, u_r.at[part, src], partner).wait_recv()
-            return state * drecv[src] + ur[src, rows_u].astype(f32)
-
-        lax.fori_loop(0, HEADS, step, jnp.zeros((TOK, KW), f32))
+            return state
+
+        lax.fori_loop(0, HEADS - 1, step, jnp.zeros((TOK, KW), f32))
         ph(f"m_w{part + 1}")
         w_pass(1, part + 1)
         w_pass(3, (part + 3) % 4)
 
     def attend(i):
         h = (sp + i) % HEADS
-        for part in range(2):
-            there = sr.at[h, pl.ds(part * TOK, TOK)]
-            remote(there, there, s_s, s_r.at[part, h], partner).wait_recv()
+
+        @pl.when(sp > 0)
+        def _():
+            for part in range(2):
+                there = sr.at[h, pl.ds(part * TOK, TOK)]
+                remote(there, there, s_s, s_r.at[part, h], partner).wait_recv()
+
         o = intra[h] + dot_t(lt[h], sr[h], 1, 1)
         ms = jnp.mean(o * o, axis=-1, keepdims=True)
         lanes = pl.ds(pl.multiple_of(h * DV, DV), DV)
@@ -321,22 +332,22 @@
     w_pass(1, 3)
     w_pass(3, 1)
     for part in range(2):
-        ph(f"m_loopC{part}")
-
-        @pl.loop(part * 4, part * 4 + 4)
-        def _(i):
-            attend(2 * i)
-
-            @pl.when(i > 0)
-            def _():
-                t_send(2 * i - 1)
-
-            attend(2 * i + 1)
-            t_send(2 * i)
-
         ph(f"m_w{part + 4}")
         w_pass(2, part)
         w_pass(2, part + 2)
+
+    ph("m_loopC")
+
+    @pl.loop(0, HEADS // 2)
+    def _(i):
+        attend(2 * i)
+
+        @pl.when(i > 0)
+        def _():
+            t_send(2 * i - 1)
+
+        attend(2 * i + 1)
+        t_send(2 * i)
 
     ph("m_twait")
     t_send(HEADS - 1)
@@ -372,13 +383,13 @@
     for n in range(8):
         lanes = pl.ds(n * 256, 256)
         res = (skipv[:, lanes].astype(f32) + pj[n].astype(f32) * r1 * bg[:, lanes]).astype(bf16)
-        res_out[:, lanes] = res
+        res_v[:, lanes] = res
         rs = res.astype(f32)
         total = total + jnp.sum(rs * rs, axis=-1, keepdims=True)
     r2 = lax.rsqrt(total * (1.0 / D) + epsilon)
     for j in range(16):
         lanes = pl.ds(j * 128, 128)
-        rf[pl.ds(j, TOK, stride=16), :] = res_out[:, lanes].astype(f32) * r2 * pg[:, lanes]
+        rf[pl.ds(j, TOK, stride=16), :] = res_v[:, lanes].astype(f32) * r2 * pg[:, lanes]
 
     @pl.loop(0, 8)
     def _(i):
@@ -387,6 +398,7 @@
         )
 
     ph("e_pack")
+    pl.semaphore_wait(ready, len(mates))
     for one in tables:
         one.wait()
 
@@ -396,30 +408,31 @@
             for u in range(4):
                 o = grp * PER + i * 4 + u
                 for k in range(CAP):
-                    xs[o * CAP + k] = x3[jnp.clip(idx[k, o], 0, TOK - 1)]
-
-    def send(grp, src, dst, s, r, place_of, sign):
-        def one(i, to, dy):
-            at = pl.ds((grp * PER + i * 4 + dy) * CAP, CAP)
-            remote(src.at[at], dst.at[at], s, r.at[grp], (to, dps[(sign * dy) % 4][grp])).start()
-
+                    xs[o * CAP + k] = x3[idx[k, o] & (TOK - 1)]
+
+    def send(grp, src, dst, s, r, sign):
         if grp == 0:
             pltpu.make_async_copy(src.at[pl.ds(0, CAP)], dst.at[pl.ds(0, CAP)], r.at[0]).start()
 
-        @pl.loop(0, HEADS if grp else HEADS - 1)
+        def eight(i, own):
+            to = ((z + sign * i + 4) % 4) * 4 + (x + sign * (i + grp) + 8) % 4
+            for dy in (2, 1, 3, 0):
+                for dc in (1, 0):
+                    if not (own and dy == 0 and dc == 0):
+                        at = pl.ds((grp * PER + i * 8 + dy * 2 + dc) * CAP, CAP)
+                        there = (to, dps[(sign * dy) % 4][dc])
+                        remote(src.at[at], dst.at[at], s, r.at[grp], there).start()
+
+        @pl.loop(0, 3 if grp == 0 else 4)
         def _(j):
-            i = HEADS - 1 - j
-            to = place_of(i)
-            for dy in (3, 2, 1, 0):
-                one(i, to, dy)
+            eight(3 - j, False)
 
         if grp == 0:
-            for dy in (3, 2, 1):
-                one(0, sp, dy)
+            eight(0, True)
 
     for grp in range(GROUPS):
         pack(grp)
-        send(grp, xs, xr, x_s, x_r, ahead, 1)
+        send(grp, xs, xr, x_s, x_r, 1)
 
     R = PER * CAP
     for grp in range(GROUPS):
@@ -467,7 +480,7 @@
             )
 
         ph(f"e_ysend{grp}")
-        send(grp, ys, yr, y_s, y_r, behind, -1)
+        send(grp, ys, yr, y_s, y_r, -1)
 
     for grp in range(GROUPS):
         ph(f"e_ywait{grp}")
@@ -480,8 +493,8 @@
     def _(i):
         for k in range(4):
             t = i * 4 + k
-            one = yr[jnp.clip(idx[CAP, t], 0, EXPERTS * CAP - 1)].astype(f32) * wts[0, t]
-            two = yr[jnp.clip(idx[CAP + 1, t], 0, EXPERTS * CAP - 1)].astype(f32) * wts[1, t]
+            one = yr[idx[CAP, t] & 511].astype(f32) * wts[0, t]
+            two = yr[idx[CAP + 1, t] & 511].astype(f32) * wts[1, t]
             rf[pl.ds(pl.multiple_of(t * 16, 16), 16), :] = one + two
 
     ph("e_norm")
@@ -492,15 +505,27 @@
     r1 = lax.rsqrt(total * (1.0 / D) + epsilon)
     for j in range(16):
         lanes = pl.ds(j * 128, 128)
-        norm_out[:, lanes] = rf[pl.ds(j, TOK, stride=16), :] * r1 * gain[:, lanes]
+        new = rf[pl.ds(j, TOK, stride=16), :] * r1 * gain[:, lanes]
+        out[:, lanes] = (res_v[:, lanes].astype(f32) + new).astype(bf16)
 
     ph("e_sendwait")
     fifteen = pl.ds(0, HEADS - 1)
     most = pl.ds(0, (EXPERTS - 1) * CAP)
     remote(spk_in.at[fifteen], spk_in.at[fifteen], spk_s, spk_r, partner).wait_send()
     remote(drecv.at[fifteen], drecv.at[fifteen], d_s, d_r, partner).wait_send()
-    remote(us.at[fifteen], ur.at[fifteen], u_s, u_r.at[0, 0], partner).wait_send()
-    remote(ss.at[fifteen], sr.at[fifteen], s_s, s_r.at[0, 0], partner).wait_send()
+    @pl.when(sp < HEADS - 1)
+    def _():
+        remote(us.at[fifteen], ur.at[fifteen], u_s, u_r.at[0, 0], partner).wait_send()
+
+    @pl.when(sp == 0)
+    def _():
+        remote(ss.at[fifteen], sr.at[fifteen], s_s, s_r.at[0, 0], partner).wait_send()
+
+    @pl.when(sp > 0)
+    def _():
+        less = pl.ds(0, HEADS - 2)
+        remote(ss.at[less], sr.at[less], s_s, s_r.at[0, 0], partner).wait_send()
+
     remote(tall.at[pl.ds(0, TOK)], tall.at[pl.ds(TOK, TOK)], t_s, t_r, partner).wait_send()
     remote(po.at[pl.ds(0, 4)], pj.at[pl.ds(0, 4)], p_s, p_r, partner).wait_send()
     remote(wall.at[pl.ds(0, 3)], wall.at[pl.ds(0, 3)], w_s, w_r.at[0, 0], partner).wait_send()
@@ -516,13 +541,11 @@
     R = PER * CAP
     return pl.pallas_call(
         layer_kernel,
-        out_shape=(
-            jax.ShapeDtypeStruct((TOK, D), bf16),
-            jax.ShapeDtypeStruct((TOK, D), f32),
-        ),
+        out_shape=jax.ShapeDtypeStruct((TOK, D), bf16),
         in_specs=[hbm] * 5 + [vmem, hbm] + [vmem] * 6 + [hbm] * 3,
-        out_specs=(vmem, vmem),
+        out_specs=vmem,
         scratch_shapes=[
+            pltpu.VMEM((TOK, D), bf16),
             pltpu.VMEM((TOK, D), bf16),
             pltpu.VMEM((TOK, D), bf16),
             pltpu.VMEM((TOK, D), bf16),
@@ -545,12 +568,12 @@
             pltpu.VMEM((2 * TOK, HEADS * DV), bf16),
             pltpu.VMEM((8, TOK, 256), bf16),
             pltpu.VMEM((4, TOK, 256), bf16),
-            pltpu.VMEM((R * 16, 128), f32),
+            pltpu.VMEM((TOK * 16, 128), f32),
             pltpu.VMEM((TOK, 16, 128), bf16),
             pltpu.VMEM((EXPERTS * CAP, 16, 128), bf16),
             pltpu.VMEM((EXPERTS * CAP, 16, 128), bf16),
             pltpu.VMEM((EXPERTS * CAP, 16, 128), bf16),
-            pltpu.VMEM((EXPERTS * CAP, 16, 128), bf16),
+            pltpu.VMEM((512, 16, 128), bf16),
             pltpu.VMEM((R, D), bf16),
             pltpu.VMEM((R, FF), bf16),
             pltpu.VMEM((D, FF), bf16),
@@ -560,6 +583,7 @@
             pltpu.VMEM((TOP, TOK), f32),
             pltpu.SMEM((8, TOK), jnp.int32),
             pltpu.SMEM((TOP, TOK), f32),
+            pltpu.SemaphoreType.REGULAR,
             dma((6,)),
             dma, dma,
             dma, dma((3, 8)),
@@ -597,7 +621,7 @@
     assigned_specialists,
     dispatcher_logits,
 ):
-    res, norm = layer(
+    out = layer(
         mapped_probe_matrix[0],
         mapped_lookup_matrix[0],
         retention_preactivation[0],
@@ -615,7 +639,7 @@
         specialist_expand_matrix[0],
         specialist_contract_matrix[0],
     )
-    return (res.astype(f32) + norm).astype(bf16)[None]
+    return out[None]
 
 
 def solution(mesh):

time: 116 us -> 111 us (0.957)
  Pallas kernels: 113 us -> 108 us
  other arithmetic: 2.26 us -> 0 us
  local copies, waits for them, and re-layouts: 0 us -> 1.88 us
    pallas_call x1, Pallas kernels: 113 us -> 108 us  [layer(): pl.pallas_call(layer_kernel, out_shape=jax.ShapeDtypeStruct((TOK, D), bf1...]
    broadcast_in_dim x1 -> x0, other arithmetic: 2.26 us -> none  [shards(): return (res.astype(f32) + norm).astype(bf16)[None]]
    unnamed x0 -> x1, local copies, waits for them, and re-layouts: none -> 1.88 us
where the time goes in v3:
time: 111 us; the launch traced here: 110 us
  Pallas kernels  108 us (97%)
  local copies, waits for them, and re-layouts  1.88 us (2%)
    pallas_call x1, Pallas kernels, layer(): pl.pallas_call(layer_kernel, out_shape=jax.ShapeDtypeStruct((TOK, D), bf1...  108 us

profile of v3, /device:TPU:1, one launch (start us, length us, event | category | flops | bytes accessed | tf_op | source)
XLA Modules:
  0.0 109.9 jit_solution(9015313494713112296)
XLA Ops:
  0.0 108.0 %layer.1 = bf16[128,2048]{1,0:T(8,128)(2,1)} custom-call(bf16[128,2048]{1,0:T(8,128)(2,1)} %bitcast.25, bf16[128,2048]{1,0:T(8,128)(2,1)} %bitcast.26, bf16[128,2048]{1,0:T(8,128)(2,1)} %bitcast.27, bf16[128,4096]{1,0:T(8,128)(2,1)} %bitcast.24, bf16[128,2048]{1,0:T(8,128)(2,1)} %bitcast.28, f32[1,2048]{1,0:T(1,128)} %bitcast.30, bf16[4096,256]{1,0:T(8,128)(2,1)} %w_h.1, ...), custom_call_target="tpu_custom_call" | custom-call | tf_op jit(solution)/shard_map/layer/pallas_call | solution.py:542
  108.0 1.9 %copy.18 = bf16[1,128,2048]{2,1,0:T(8,128)(2,1)} copy(bf16[1,128,2048]{2,1,0:T(8,128)(2,1)} %bitcast.23) | data formatting | bytes 1048576

commit v4 on v3

--- a/solution.py
+++ b/solution.py
@@ -17,8 +17,9 @@
 EXPERTS = 128
 PIECE = 512
 HALF = 64
-GROUPS = 4
+GROUPS = 2
 PER = EXPERTS // GROUPS
+UNROLL = 4
 
 epsilon = 1e-06
 f32 = jnp.float32
@@ -27,6 +28,20 @@
 
 def dot_t(a, b, ca, cb):
     return lax.dot_general(a, b, (((ca,), (cb,)), ((), ())), preferred_element_type=f32)
+
+
+def steps_of(o):
+    return [min(v, 4 - v) for v in o[:3]]
+
+
+def far_first_offsets():
+    every = [
+        (dz, dx, dy, dc) for dz in range(4) for dx in range(4) for dy in range(4) for dc in range(2)
+    ]
+    return sorted(every, key=lambda o: (-sum(steps_of(o)), -o[3], steps_of(o), o))
+
+
+OFFSETS = far_first_offsets()
 
 
 def phases():
@@ -44,7 +59,7 @@
 
 
 def layer_kernel(
-    q_h, k_h, g_h, v_h, skip_h, spk, w_h, gs, bg, pg, chosen, logits, gain, wg_h, wu_h, wd_h,
+    q_h, k_h, g_h, v_h, skip_h, spk, w_h, gs, bg, pg, chosen, logits, ranked, gain, wg_h, wu_h, wd_h,
     out,
     res_v, qv, kv, gv, vv, skipv, spk_in, wall,
     bgs, lf, lw, ca, lt, intra, us, ur, dsend, drecv, ss, sr, tall, pj, po, rf,
@@ -121,8 +136,7 @@
             spk.at[:, pl.ds(pl.multiple_of(to * TOK, TOK), TOK)], spk_in.at[sp], spk_s, spk_r, (to, dp)
         ).start()
 
-    base = ((x + z) % 2) * 4
-    obase = 4 - base
+    par = (x + z) % 2
     up = (sp, dps[1][0])
     down = (sp, dps[3][0])
     around = [(ahead(1), dp), (ahead(3), dp), (ahead(4), dp), (ahead(12), dp)]
@@ -130,24 +144,47 @@
     def rows(piece):
         return pl.ds(pl.multiple_of(piece * PIECE, PIECE), PIECE)
 
-    for i in range(4):
-        a, b = base + i, base + (i + 2) % 4
-        remote(w_h.at[rows(a)], wall.at[1, rows(a)], w_s, w_r.at[0, a], up).start()
-        remote(w_h.at[rows(b)], wall.at[3, rows(b)], w_s, w_r.at[2, b], down).start()
+    def mine(m):
+        return par * 7 + (1 - 2 * par) * m
+
+    def theirs(m):
+        return 7 - mine(m)
+
+    def w_up(m):
+        at = rows(mine(m))
+        remote(w_h.at[at], wall.at[1, at], w_s, w_r.at[0, mine(m)], up).start()
+
+    def w_down(m):
+        at = rows(mine(m))
+        remote(w_h.at[at], wall.at[3, at], w_s, w_r.at[2, mine(m)], down).start()
+
+    for m in (0, 1, 2):
+        w_up(m)
+    for m in (2, 3, 0):
+        w_down(m)
 
     def w_wait(slot, piece):
         there = wall.at[slot, rows(piece)]
         remote(there, there, w_s, w_r.at[slot - 1, piece], partner).wait_recv()
 
-    def w_pass(slot, i):
-        piece = base + i
-        w_wait(slot, piece)
-        there = wall.at[slot, rows(piece)]
-        if slot == 1 and i < 2:
-            remote(there, wall.at[2, rows(piece)], w_s, w_r.at[1, piece], up).start()
-        if slot == 3 and i >= 2:
-            remote(there, wall.at[2, rows(piece)], w_s, w_r.at[1, piece], down).start()
-        remote(there, there, w_s, w_r.at[slot - 1, piece], around[i]).start()
+    def w_share(slot, m):
+        for k in range(4):
+            quarter = PIECE // 4
+            at = pl.ds(pl.multiple_of(mine(m) * PIECE + k * quarter, quarter), quarter)
+            some = wall.at[slot, at]
+            remote(some, some, w_s, w_r.at[slot - 1, mine(m)], around[k]).start()
+
+    def w_early(m):
+        for slot, n, to in ((1, m, up), (3, m + 2, down)):
+            w_wait(slot, mine(n))
+            at = rows(mine(n))
+            remote(wall.at[slot, at], wall.at[2, at], w_s, w_r.at[1, mine(n)], to).start()
+            if n < 3:
+                w_share(slot, n)
+
+    def w_pass(slot, m):
+        w_wait(slot, mine(m))
+        w_share(slot, m)
 
     ph("m_decay")
     loads[0].wait()
@@ -164,12 +201,13 @@
     ph("m_route")
     esp, edp = chosen[...] >> 3, chosen[...] & 7
     off = (
-        (((esp & 3) - (esp >> 2) + 8 - x + z) & 3) * 32
-        + (((esp >> 2) + 4 - z) & 3) * 8
+        (((esp >> 2) + 4 - z) & 3) * 32
+        + (((esp & 3) + 4 - x) & 3) * 8
         + (((edp >> 1) + 4 - y) & 3) * 2
         + (((edp & 1) + c) & 1)
-    )
-    pick = [jnp.where(row == off[r : r + 1], 1.0, 0.0) for r in range(TOP)]
+    ).astype(f32)
+    offset_of = jnp.broadcast_to(ranked[...], (EXPERTS, TOK)).T
+    pick = [jnp.where(offset_of == off[r : r + 1], 1.0, 0.0) for r in range(TOP)]
     named = pick[0] + pick[1]
     later = jnp.where(row < col, 1.0, 0.0).astype(bf16)
     rank = dot_t(named.astype(bf16), later, 1, 0)
@@ -198,6 +236,12 @@
     remote(spk_in.at[pl.ds(0, HEADS)], spk_in.at[pl.ds(0, HEADS)], spk_s, spk_r, partner).wait_recv()
     ph("m_loopA")
 
+    def far_first(m):
+        return (2 + m) * (1 - m // 2) + (3 - m) * (m // 2)
+
+    def around_of(n):
+        return ((z + far_first(n // 4)) % 4) * 4 + (x + far_first(n % 4)) % 4
+
     def u_send(h, part):
         if part == 0:
             remote(dsend.at[h], drecv.at[sp], d_s, d_r, (h, dp)).start()
@@ -225,16 +269,16 @@
         ca[h] = carried.astype(bf16)
         lt[h] = (lifted * jnp.where(first, 1.0, jnp.exp(e1))).astype(bf16)
 
-    @pl.loop(0, HEADS // 2)
-    def _(i):
-        for k in range(2):
-            form((sp + 1 + 2 * i + k) % HEADS)
-
-        u_send((sp + 1 + 2 * i) % HEADS, 0)
-
-        @pl.when(i < HEADS // 2 - 1)
+    @pl.loop(0, HEADS // UNROLL)
+    def _(i):
+        for k in range(UNROLL):
+            form(around_of(UNROLL * i + k))
+        for k in range(UNROLL - 1):
+            u_send(around_of(UNROLL * i + k), 0)
+
+        @pl.when(i < HEADS // UNROLL - 1)
         def _():
-            u_send((sp + 2 + 2 * i) % HEADS, 0)
+            u_send(around_of(UNROLL * i + UNROLL - 1), 0)
 
     ph("m_sendB")
 
@@ -252,9 +296,9 @@
 
     pltpu.make_async_copy(dsend.at[sp], drecv.at[sp], d_r).start()
 
-    @pl.loop(1, HEADS)
-    def _(i):
-        u_send((sp + i) % HEADS, 1)
+    @pl.loop(0, HEADS - 1)
+    def _(i):
+        u_send(around_of(i), 1)
 
     for one in tables:
         one.start()
@@ -279,8 +323,7 @@
             intra[h] = dot_t(scores.astype(bf16), vh, 1, 0)
 
     ph("m_w0")
-    w_pass(1, 0)
-    w_pass(3, 2)
+    w_early(0)
     ph("m_dwait")
     remote(drecv.at[pl.ds(0, HEADS)], drecv.at[pl.ds(0, HEADS)], d_s, d_r, partner).wait_recv()
 
@@ -307,18 +350,24 @@
 
         lax.fori_loop(0, HEADS - 1, step, jnp.zeros((TOK, KW), f32))
         ph(f"m_w{part + 1}")
-        w_pass(1, part + 1)
-        w_pass(3, (part + 3) % 4)
+        if part == 0:
+            w_early(1)
+            w_up(3)
+            w_up(4)
+            w_down(1)
+            w_down(4)
+        else:
+            w_pass(1, 2)
+            w_pass(3, 0)
+
+    def arrived(i):
+        h = (sp + i) % HEADS
+        for part in range(2):
+            there = sr.at[h, pl.ds(part * TOK, TOK)]
+            remote(there, there, s_s, s_r.at[part, h], partner).wait_recv()
 
     def attend(i):
         h = (sp + i) % HEADS
-
-        @pl.when(sp > 0)
-        def _():
-            for part in range(2):
-                there = sr.at[h, pl.ds(part * TOK, TOK)]
-                remote(there, there, s_s, s_r.at[part, h], partner).wait_recv()
-
         o = intra[h] + dot_t(lt[h], sr[h], 1, 1)
         ms = jnp.mean(o * o, axis=-1, keepdims=True)
         lanes = pl.ds(pl.multiple_of(h * DV, DV), DV)
@@ -329,25 +378,31 @@
         remote(tall.at[pl.ds(0, TOK), lanes], tall.at[pl.ds(TOK, TOK), lanes], t_s, t_r, partner).start()
 
     ph("m_w3")
-    w_pass(1, 3)
+    w_pass(2, 0)
+    w_pass(2, 2)
+    ph("m_w4")
+    w_pass(2, 1)
+    w_pass(2, 3)
+    ph("m_w5")
     w_pass(3, 1)
-    for part in range(2):
-        ph(f"m_w{part + 4}")
-        w_pass(2, part)
-        w_pass(2, part + 2)
-
     ph("m_loopC")
 
-    @pl.loop(0, HEADS // 2)
-    def _(i):
-        attend(2 * i)
+    @pl.loop(0, HEADS // UNROLL)
+    def _(i):
+        @pl.when(sp > 0)
+        def _():
+            for k in range(UNROLL):
+                arrived(UNROLL * i + k)
+
+        for k in range(UNROLL):
+            attend(UNROLL * i + k)
 
         @pl.when(i > 0)
         def _():
-            t_send(2 * i - 1)
-
-        attend(2 * i + 1)
-        t_send(2 * i)
+            t_send(UNROLL * i - 1)
+
+        for k in range(UNROLL - 1):
+            t_send(UNROLL * i + k)
 
     ph("m_twait")
     t_send(HEADS - 1)
@@ -364,10 +419,14 @@
 
     ph("m_proj0")
     project(0)
-    for slot in (1, 3, 2):
+    for slot in (2, 1, 3):
         ph(f"m_ow{slot}")
-        for i in range(4):
-            w_wait(slot, obase + i)
+        for m in range(4 if slot == 2 else 3):
+            w_wait(slot, theirs(m))
+        if slot == 1:
+            w_wait(1, mine(3))
+        if slot != 2:
+            w_wait(slot, mine(4))
         ph(f"m_proj{slot}")
         project(slot)
     ph("m_pwait")
@@ -411,40 +470,33 @@
                     xs[o * CAP + k] = x3[idx[k, o] & (TOK - 1)]
 
     def send(grp, src, dst, s, r, sign):
-        if grp == 0:
-            pltpu.make_async_copy(src.at[pl.ds(0, CAP)], dst.at[pl.ds(0, CAP)], r.at[0]).start()
-
-        def eight(i, own):
-            to = ((z + sign * i + 4) % 4) * 4 + (x + sign * (i + grp) + 8) % 4
-            for dy in (2, 1, 3, 0):
-                for dc in (1, 0):
-                    if not (own and dy == 0 and dc == 0):
-                        at = pl.ds((grp * PER + i * 8 + dy * 2 + dc) * CAP, CAP)
-                        there = (to, dps[(sign * dy) % 4][dc])
-                        remote(src.at[at], dst.at[at], s, r.at[grp], there).start()
-
-        @pl.loop(0, 3 if grp == 0 else 4)
-        def _(j):
-            eight(3 - j, False)
-
-        if grp == 0:
-            eight(0, True)
+        zs = [(z + sign * i + 4) % 4 * 4 for i in range(4)]
+        xo = [(x + sign * i + 4) % 4 for i in range(4)]
+        for o in range(grp * PER, grp * PER + PER):
+            dz, dx, dy, dc = OFFSETS[o]
+            at = pl.ds(o * CAP, CAP)
+            if o < EXPERTS - 1:
+                there = (zs[dz] + xo[dx], dps[(sign * dy) % 4][dc])
+                remote(src.at[at], dst.at[at], s, r, there).start()
+            else:
+                pltpu.make_async_copy(src.at[at], dst.at[at], r).start()
 
     for grp in range(GROUPS):
         pack(grp)
-        send(grp, xs, xr, x_s, x_r, 1)
+        send(grp, xs, xr, x_s, x_r.at[grp], 1)
 
     R = PER * CAP
     for grp in range(GROUPS):
+        low = grp * R
         ph(f"e_xwait{grp}")
         at = pl.ds(grp * R, R)
         remote(xr.at[at], xr.at[at], x_s, x_r.at[grp], partner).wait_recv()
         ph(f"e_relay{grp}")
 
         @pl.loop(0, R // 12)
-        def _(i):
+        def _(i, low=low):
             rf[pl.ds(pl.multiple_of(i * 192, 192), 192), :] = (
-                xr[pl.ds(grp * R + i * 12, 12)].astype(f32).reshape(192, 128)
+                xr[pl.ds(low + i * 12, 12)].astype(f32).reshape(192, 128)
             )
 
         for j in range(16):
@@ -474,13 +526,13 @@
         ph(f"e_yrelay{grp}")
 
         @pl.loop(0, R // 12)
-        def _(i):
-            ys[pl.ds(grp * R + i * 12, 12)] = (
+        def _(i, low=low):
+            ys[pl.ds(low + i * 12, 12)] = (
                 rf[pl.ds(pl.multiple_of(i * 192, 192), 192), :].reshape(12, 16, 128).astype(bf16)
             )
 
         ph(f"e_ysend{grp}")
-        send(grp, ys, yr, y_s, y_r, -1)
+        send(grp, ys, yr, y_s, y_r.at[grp], -1)
 
     for grp in range(GROUPS):
         ph(f"e_ywait{grp}")
@@ -542,7 +594,7 @@
     return pl.pallas_call(
         layer_kernel,
         out_shape=jax.ShapeDtypeStruct((TOK, D), bf16),
-        in_specs=[hbm] * 5 + [vmem, hbm] + [vmem] * 6 + [hbm] * 3,
+        in_specs=[hbm] * 5 + [vmem, hbm] + [vmem] * 7 + [hbm] * 3,
         out_specs=vmem,
         scratch_shapes=[
             pltpu.VMEM((TOK, D), bf16),
@@ -568,7 +620,7 @@
             pltpu.VMEM((2 * TOK, HEADS * DV), bf16),
             pltpu.VMEM((8, TOK, 256), bf16),
             pltpu.VMEM((4, TOK, 256), bf16),
-            pltpu.VMEM((TOK * 16, 128), f32),
+            pltpu.VMEM((R * 16, 128), f32),
             pltpu.VMEM((TOK, 16, 128), bf16),
             pltpu.VMEM((EXPERTS * CAP, 16, 128), bf16),
             pltpu.VMEM((EXPERTS * CAP, 16, 128), bf16),
@@ -634,6 +686,7 @@
         specialist_prenormal_scale.reshape(1, -1),
         assigned_specialists[0].T,
         dispatcher_logits[0].T,
+        jnp.array([[dz * 32 + dx * 8 + dy * 2 + dc for dz, dx, dy, dc in OFFSETS]], f32),
         specialist_branch_scale.reshape(1, -1),
         specialist_switch_matrix[0],
         specialist_expand_matrix[0],

time: 111 us -> 106 us (0.955)
  Pallas kernels: 108 us -> 104 us
    pallas_call x1, Pallas kernels: 108 us -> 104 us  [layer(): pl.pallas_call(layer_kernel, out_shape=jax.ShapeDtypeStruct((TOK, D), bf1...]
where the time goes in v4:
time: 106 us
  Pallas kernels  104 us (98%)
  local copies, waits for them, and re-layouts  1.88 us (2%)
    pallas_call x1, Pallas kernels, layer(): pl.pallas_call(layer_kernel, out_shape=jax.ShapeDtypeStruct((TOK, D), bf1...  104 us

profile of v4, /device:TPU:1, one launch (start us, length us, event | category | flops | bytes accessed | tf_op | source)
XLA Modules:
  0.0 106.0 jit_solution(8657591761416782874)
XLA Ops:
  0.0 104.1 %layer.1 = bf16[128,2048]{1,0:T(8,128)(2,1)} custom-call(bf16[128,2048]{1,0:T(8,128)(2,1)} %bitcast.25, bf16[128,2048]{1,0:T(8,128)(2,1)} %bitcast.26, bf16[128,2048]{1,0:T(8,128)(2,1)} %bitcast.27, bf16[128,4096]{1,0:T(8,128)(2,1)} %bitcast.24, bf16[128,2048]{1,0:T(8,128)(2,1)} %bitcast.28, f32[1,2048]{1,0:T(1,128)} %bitcast.30, bf16[4096,256]{1,0:T(8,128)(2,1)} %w_h.1, ...), custom_call_target="tpu_custom_call" | custom-call | tf_op jit(solution)/shard_map/layer/pallas_call | solution.py:594
  104.1 1.9 %copy.19 = bf16[1,128,2048]{2,1,0:T(8,128)(2,1)} copy(bf16[1,128,2048]{2,1,0:T(8,128)(2,1)} %bitcast.23) | data formatting | bytes 1048576

commit v5 on v4

--- a/solution.py
+++ b/solution.py
@@ -17,8 +17,9 @@
 EXPERTS = 128
 PIECE = 512
 HALF = 64
-GROUPS = 2
-PER = EXPERTS // GROUPS
+SIZES = (32, 48, 48)
+ORDER = (1, 3, 2)
+LAST = (1, 3, 2)
 UNROLL = 4
 
 epsilon = 1e-06
@@ -63,7 +64,7 @@
     out,
     res_v, qv, kv, gv, vv, skipv, spk_in, wall,
     bgs, lf, lw, ca, lt, intra, us, ur, dsend, drecv, ss, sr, tall, pj, po, rf,
-    x3, xs, xr, ys, yr, xm, hs, wg, wu, wd, idx_v, wts_v, idx, wts,
+    part_sum, x3, xs, xr, ys, yr, xm, hs, wg, wu, wd, idx_v, wts_v, idx, wts,
     ready, lsem, spk_s, spk_r, w_s, w_r, u_s, u_r, d_s, d_r, s_s, s_r, t_s, t_r, p_s, p_r,
     esem, isem, x_s, x_r, y_s, y_r,
 ):
@@ -383,8 +384,6 @@
     ph("m_w4")
     w_pass(2, 1)
     w_pass(2, 3)
-    ph("m_w5")
-    w_pass(3, 1)
     ph("m_loopC")
 
     @pl.loop(0, HEADS // UNROLL)
@@ -404,31 +403,54 @@
         for k in range(UNROLL - 1):
             t_send(UNROLL * i + k)
 
+    ph("m_w5")
+    w_pass(3, 1)
     ph("m_twait")
     t_send(HEADS - 1)
     loads[4].wait()
     loads[5].wait()
     remote(tall.at[pl.ds(0, TOK)], tall.at[pl.ds(TOK, TOK)], t_s, t_r, partner).wait_recv()
 
-    def project(slot):
-        acc = jnp.dot(tall[...], wall[slot], preferred_element_type=f32).astype(bf16)
+    def pieces_dot(slot, pieces):
+        total = None
+        for piece in pieces:
+            at = rows(piece)
+            term = jnp.dot(tall[:, at], wall[slot, at], preferred_element_type=f32)
+            total = term if total is None else total + term
+        return total
+
+    def hand_out(slot, acc):
+        acc = acc.astype(bf16)
         shard = ((y + 4 - slot) % 4) * 2 + c
         po[slot] = acc[TOK:]
         pj[shard] = acc[:TOK]
         remote(po.at[slot], pj.at[shard], p_s, p_r, partner).start()
 
     ph("m_proj0")
-    project(0)
-    for slot in (2, 1, 3):
+    hand_out(0, jnp.dot(tall[...], wall[0], preferred_element_type=f32))
+    late = {1: [mine(4)], 2: [theirs(1), theirs(3)], 3: [mine(4), theirs(1)]}
+    soon = {
+        1: [mine(0), mine(1), mine(2), mine(3), theirs(0), theirs(1), theirs(2)],
+        2: [mine(0), mine(1), mine(2), mine(3), theirs(0), theirs(2)],
+        3: [mine(0), mine(1), mine(2), mine(3), theirs(0), theirs(2)],
+    }
+    waits = {
+        1: [mine(3), theirs(0), theirs(1), theirs(2)],
+        2: [theirs(0), theirs(2)],
+        3: [theirs(0), theirs(2)],
+    }
+    for slot in ORDER:
         ph(f"m_ow{slot}")
-        for m in range(4 if slot == 2 else 3):
-            w_wait(slot, theirs(m))
-        if slot == 1:
-            w_wait(1, mine(3))
-        if slot != 2:
-            w_wait(slot, mine(4))
+        for piece in waits[slot]:
+            w_wait(slot, piece)
         ph(f"m_proj{slot}")
-        project(slot)
+        part_sum[slot - 1] = pieces_dot(slot, soon[slot])
+    for slot in LAST:
+        ph(f"m_lw{slot}")
+        for piece in late[slot]:
+            w_wait(slot, piece)
+        ph(f"m_last{slot}")
+        hand_out(slot, part_sum[slot - 1] + pieces_dot(slot, late[slot]))
     ph("m_pwait")
     remote(po.at[pl.ds(0, 4)], pj.at[pl.ds(0, 4)], p_s, p_r, partner).wait_recv()
 
@@ -461,18 +483,23 @@
     for one in tables:
         one.wait()
 
+    first = [sum(SIZES[:grp]) for grp in range(len(SIZES))]
+
+    def span(grp):
+        return pl.ds(first[grp] * CAP, SIZES[grp] * CAP)
+
     def pack(grp):
-        @pl.loop(0, PER // 4)
+        @pl.loop(0, SIZES[grp] // 4)
         def _(i):
             for u in range(4):
-                o = grp * PER + i * 4 + u
+                o = first[grp] + i * 4 + u
                 for k in range(CAP):
                     xs[o * CAP + k] = x3[idx[k, o] & (TOK - 1)]
 
     def send(grp, src, dst, s, r, sign):
         zs = [(z + sign * i + 4) % 4 * 4 for i in range(4)]
         xo = [(x + sign * i + 4) % 4 for i in range(4)]
-        for o in range(grp * PER, grp * PER + PER):
+        for o in range(first[grp], first[grp] + SIZES[grp]):
             dz, dx, dy, dc = OFFSETS[o]
             at = pl.ds(o * CAP, CAP)
             if o < EXPERTS - 1:
@@ -481,15 +508,15 @@
             else:
                 pltpu.make_async_copy(src.at[at], dst.at[at], r).start()
 
-    for grp in range(GROUPS):
+    for grp in range(len(SIZES)):
         pack(grp)
         send(grp, xs, xr, x_s, x_r.at[grp], 1)
 
-    R = PER * CAP
-    for grp in range(GROUPS):
-        low = grp * R
+    for grp in range(len(SIZES)):
+        R = SIZES[grp] * CAP
+        low = first[grp] * CAP
         ph(f"e_xwait{grp}")
-        at = pl.ds(grp * R, R)
+        at = span(grp)
         remote(xr.at[at], xr.at[at], x_s, x_r.at[grp], partner).wait_recv()
         ph(f"e_relay{grp}")
 
@@ -500,26 +527,26 @@
             )
 
         for j in range(16):
-            xm[:, pl.ds(j * 128, 128)] = rf[pl.ds(j, R, stride=16), :].astype(bf16)
+            xm[pl.ds(0, R), pl.ds(j * 128, 128)] = rf[pl.ds(j, R, stride=16), :].astype(bf16)
         ph(f"e_mlp{grp}")
         if grp == 0:
             experts_in[0].wait()
             experts_in[1].wait()
 
         @pl.loop(0, FF // 256)
-        def _(n):
+        def _(n, R=R):
             lanes = pl.ds(pl.multiple_of(n * 256, 256), 256)
-            a = jnp.dot(xm[...], wg[:, lanes], preferred_element_type=f32)
-            b = jnp.dot(xm[...], wu[:, lanes], preferred_element_type=f32)
-            hs[:, lanes] = (a * (1.0 / (1.0 + jnp.exp(-a))) * b).astype(bf16)
+            a = jnp.dot(xm[pl.ds(0, R), :], wg[:, lanes], preferred_element_type=f32)
+            b = jnp.dot(xm[pl.ds(0, R), :], wu[:, lanes], preferred_element_type=f32)
+            hs[pl.ds(0, R), lanes] = (a * (1.0 / (1.0 + jnp.exp(-a))) * b).astype(bf16)
 
         if grp == 0:
             experts_in[2].wait()
 
         @pl.loop(0, D // 256)
-        def _(n):
+        def _(n, R=R):
             lanes = pl.ds(pl.multiple_of(n * 256, 256), 256)
-            a = jnp.dot(hs[...], wd[:, lanes], preferred_element_type=f32)
+            a = jnp.dot(hs[pl.ds(0, R), :], wd[:, lanes], preferred_element_type=f32)
             rf[pl.ds(2 * n, R, stride=16), :] = a[:, :128]
             rf[pl.ds(2 * n + 1, R, stride=16), :] = a[:, 128:]
 
@@ -534,9 +561,9 @@
         ph(f"e_ysend{grp}")
         send(grp, ys, yr, y_s, y_r.at[grp], -1)
 
-    for grp in range(GROUPS):
+    for grp in range(len(SIZES)):
         ph(f"e_ywait{grp}")
-        at = pl.ds(grp * R, R)
+        at = span(grp)
         remote(yr.at[at], yr.at[at], y_s, y_r.at[grp], partner).wait_recv()
 
     ph("e_comb")
@@ -590,7 +617,7 @@
     hbm = pl.BlockSpec(memory_space=pl.ANY)
     vmem = pl.BlockSpec(memory_space=pltpu.VMEM)
     dma = pltpu.SemaphoreType.DMA
-    R = PER * CAP
+    R = max(SIZES) * CAP
     return pl.pallas_call(
         layer_kernel,
         out_shape=jax.ShapeDtypeStruct((TOK, D), bf16),
@@ -621,6 +648,7 @@
             pltpu.VMEM((8, TOK, 256), bf16),
             pltpu.VMEM((4, TOK, 256), bf16),
             pltpu.VMEM((R * 16, 128), f32),
+            pltpu.VMEM((3, 2 * TOK, 256), f32),
             pltpu.VMEM((TOK, 16, 128), bf16),
             pltpu.VMEM((EXPERTS * CAP, 16, 128), bf16),
             pltpu.VMEM((EXPERTS * CAP, 16, 128), bf16),
@@ -645,8 +673,8 @@
             dma, dma,
             dma, dma,
             dma((3,)), dma((2,)),
-            dma, dma((GROUPS,)),
-            dma, dma((GROUPS,)),
+            dma, dma((len(SIZES),)),
+            dma, dma((len(SIZES),)),
         ],
         compiler_params=pltpu.CompilerParams(
             collective_id=0, has_side_effects=True, vmem_limit_bytes=58 * 2**20

time: 106 us -> 101 us (0.953)
  Pallas kernels: 104 us -> 99 us
    pallas_call x1, Pallas kernels: 104 us -> 99 us  [layer(): pl.pallas_call(layer_kernel, out_shape=jax.ShapeDtypeStruct((TOK, D), bf1...]
where the time goes in v5:
time: 101 us
  Pallas kernels  99 us (98%)
  local copies, waits for them, and re-layouts  1.88 us (2%)
    pallas_call x1, Pallas kernels, layer(): pl.pallas_call(layer_kernel, out_shape=jax.ShapeDtypeStruct((TOK, D), bf1...  99 us

profile of v5, /device:TPU:1, one launch (start us, length us, event | category | flops | bytes accessed | tf_op | source)
XLA Modules:
  0.0 100.9 jit_solution(13906328394464274274)
XLA Ops:
  0.0 99.0 %layer.1 = bf16[128,2048]{1,0:T(8,128)(2,1)} custom-call(bf16[128,2048]{1,0:T(8,128)(2,1)} %bitcast.25, bf16[128,2048]{1,0:T(8,128)(2,1)} %bitcast.26, bf16[128,2048]{1,0:T(8,128)(2,1)} %bitcast.27, bf16[128,4096]{1,0:T(8,128)(2,1)} %bitcast.24, bf16[128,2048]{1,0:T(8,128)(2,1)} %bitcast.28, f32[1,2048]{1,0:T(1,128)} %bitcast.30, bf16[4096,256]{1,0:T(8,128)(2,1)} %w_h.1, ...), custom_call_target="tpu_custom_call" | custom-call | tf_op jit(solution)/shard_map/layer/pallas_call | solution.py:621
  99.0 1.9 %copy.19 = bf16[1,128,2048]{2,1,0:T(8,128)(2,1)} copy(bf16[1,128,2048]{2,1,0:T(8,128)(2,1)} %bitcast.23) | data formatting | bytes 1048576
